TPU v7x, 32 devices: a whole 2x2x4 slice. The times are simulated.
32 devices in a mesh: sp: 8 (over z, y), tp: 4 (over x, core).
Axes of the slice: x: 2, y: 2, z: 4, core: 2. Of those that a mesh axis runs over, the one named last changes fastest.
Arguments:
- queries: bfloat16 [1024, 2048], P('sp', 'tp'), may hold values from -6 to 6
- keys: bfloat16 [1024, 512], P('sp', 'tp'), may hold values from -6 to 6
- values: bfloat16 [1024, 512], P('sp', 'tp'), may hold values from -6 to 6
- query_gain: float32 [128], replicated, may hold values from 0.3 to 7
- key_norm_gain: float32 [128], replicated, may hold values from 0.3 to 7
- out_weight: bfloat16 [2048, 2048], P('tp'), may hold values from -0.25 to 0.25
- residual: bfloat16 [1024, 2048], P(('sp', 'tp')), may hold values from -6 to 6
- norm_gain: float32 [2048], replicated, may hold values from 0.1 to 1.9
- expert_gate: bfloat16 [8, 2048, 3072], P('sp', None, 'tp'), may hold values from -0.125 to 0.125
- expert_up: bfloat16 [8, 2048, 3072], P('sp', None, 'tp'), may hold values from -0.125 to 0.125
- expert_down: bfloat16 [8, 3072, 2048], P('sp', 'tp'), may hold values from -0.109375 to 0.109375
- routes: int32 [1024, 2], P(('sp', 'tp')), may hold values from 0 to 7, all different within a row; in each aligned block of 32 rows (0 to 31, 32 to 63, ...) at most 16 rows name the same one
- route_weight: float32 [1024, 2], P(('sp', 'tp')), may hold values from 0.25 to 1
Outputs:
- mixed: bfloat16 [1024, 2048], P(('sp', 'tp'))
Inputs may be any that keep to these rules, and one draw needn't show every extreme that they name: The two experts of a token differ. In each aligned block of 32 tokens (the tokens of one device), no expert is named by more than 16 routes, and in some block one expert is named by exactly 16.
All inputs are finite; a program needn't handle non-finite values.
Results may differ from a plain program's by a relative error of at most 0.013.
The roundings to bfloat16 on the way count: a program that leaves them out, or rounds other values in their place, can miss the bound.
Values may be sent and summed in bfloat16 or wider, within the bound.
No kernel may reach another device: no remote copies, remote signals or barrier semaphores. Data moves between devices by JAX's collectives and lax.ppermute only.
A program may use at most 64 MiB of HBM per device.

v0:
```python
import functools
import math

import jax
import jax.numpy as jnp
from jax import lax
from jax.experimental import pallas as pl
from jax.experimental.pallas import tpu as pltpu
from jax.sharding import PartitionSpec as P


HEAD_SIZE = 128
GRID_W = 64
norm_eps = 1e-06
theta_base = 10000.0


F32 = jnp.float32
BF16 = jnp.bfloat16
VM = pl.BlockSpec(memory_space=pltpu.VMEM)
SM = pl.BlockSpec(memory_space=pltpu.SMEM)
HBM = pl.BlockSpec(memory_space=pltpu.MemorySpace.HBM)


def params(mib):
    return pltpu.CompilerParams(vmem_limit_bytes=mib * 1024 * 1024)


def swap(x, axis, k):
    n = lax.axis_size(axis)
    return lax.ppermute(x, axis, [(i, i ^ k) for i in range(n)])


def call(kernel, operands, ins, outs, shapes, scratch=(), mib=4):
    operands = [
        pltpu.with_memory_space_constraint(x, pltpu.MemorySpace.HBM) if spec is HBM else x
        for x, spec in zip(operands, ins)
    ]
    return pl.pallas_call(
        kernel,
        out_shape=shapes,
        in_specs=ins,
        out_specs=outs,
        scratch_shapes=list(scratch),
        compiler_params=params(mib),
    )(*operands)


def rotate_norm(x, gain, cosine, sine):
    ms = jnp.mean(x * x, axis=-1, keepdims=True)
    v = x * lax.rsqrt(ms + norm_eps) * gain
    lane = lax.broadcasted_iota(jnp.int32, v.shape, 1)
    quarter = HEAD_SIZE // 4
    turned = jnp.where(
        (lane & (2 * quarter - 1)) < quarter,
        -pltpu.roll(v, HEAD_SIZE - quarter, 1),
        pltpu.roll(v, quarter, 1),
    )
    return v * cosine + turned * sine


def fetch(pairs, sem):
    copies = [pltpu.make_async_copy(src, dst, sem.at[i]) for i, (src, dst) in enumerate(pairs)]
    for c in copies:
        c.start()
    return copies


def key_kernel(sp_ref, gain_ref, k_ref, v_ref, kv_ref, cos_ref, sin_ref, k_scr, g_scr, sem):
    kw = k_scr.shape[1]
    copies = fetch(
        ((k_ref, k_scr), (gain_ref, g_scr), (v_ref, kv_ref.at[:, pl.ds(kw, kw)])), sem
    )
    rows = k_scr.shape[0]
    pos = sp_ref[0] * rows + lax.broadcasted_iota(jnp.int32, (rows, HEAD_SIZE), 0)
    lane = lax.broadcasted_iota(jnp.int32, (rows, HEAD_SIZE), 1)
    shift = GRID_W.bit_length() - 1
    coord = jnp.where(lane < HEAD_SIZE // 2, pos >> shift, pos & (GRID_W - 1)).astype(F32)
    freq = (lane & (HEAD_SIZE // 4 - 1)).astype(F32)
    angles = coord * jnp.exp(freq * (-2.0 * math.log(theta_base) / (HEAD_SIZE // 2)))
    cosine = jnp.cos(angles)
    sine = jnp.sin(angles)
    cos_ref[...] = cosine
    sin_ref[...] = sine
    copies[0].wait()
    copies[1].wait()
    for h in range(kw // HEAD_SIZE):
        cols = slice(h * HEAD_SIZE, (h + 1) * HEAD_SIZE)
        kv_ref[:, cols] = rotate_norm(
            k_scr[:, cols].astype(F32), g_scr[...], cosine, sine
        ).astype(BF16)
    copies[2].wait()


def query_kernel(cos_ref, sin_ref, gain_ref, q_ref, w_ref, out_ref, w_out, q_scr, g_scr, sem):
    copies = fetch(((q_ref, q_scr), (gain_ref, g_scr), (w_ref, w_out)), sem)
    rows = q_scr.shape[0]
    copies[0].wait()
    copies[1].wait()
    for h in range(q_scr.shape[1] // HEAD_SIZE):
        out_ref[h * rows : (h + 1) * rows, :] = rotate_norm(
            q_scr[:, h * HEAD_SIZE : (h + 1) * HEAD_SIZE].astype(F32),
            g_scr[...],
            cos_ref[...],
            sin_ref[...],
        ).astype(BF16)
    copies[2].wait()


def attention_kernel(npieces, tp_size, tp_ref, q_ref, w_ref, *rest):
    kv_refs = rest[:npieces]
    keep_ref, send_ref, s_scr, att_scr = rest[npieces:]
    kw = kv_refs[0].shape[1] // 2
    key_heads = kw // HEAD_SIZE
    rows = att_scr.shape[0]
    heads = q_ref.shape[0] // rows
    members = heads // key_heads
    piece = kv_refs[0].shape[0]
    scale = math.log2(math.e) / math.sqrt(HEAD_SIZE)
    pair = 2 if npieces % 2 == 0 else 1
    span = pair * piece

    def load(i, col):
        return jnp.concatenate(
            [kv_refs[i * pair + j][:, col : col + HEAD_SIZE] for j in range(pair)], axis=0
        )

    for h in range(heads):
        kc = (h // members) * HEAD_SIZE
        q = q_ref[h * rows : (h + 1) * rows, :]
        top = None
        for i in range(npieces // pair):
            s = lax.dot_general(
                q, load(i, kc), (((1,), (1,)), ((), ())), preferred_element_type=F32
            )
            s_scr[:, i * span : (i + 1) * span] = s
            top = s if top is None else jnp.maximum(top, s)
        m = jnp.max(top, axis=-1, keepdims=True) * scale
        total = None
        acc = None
        for i in range(npieces // pair):
            p = jnp.exp2(s_scr[:, i * span : (i + 1) * span] * scale - m)
            total = p if total is None else total + p
            o = jnp.dot(p.astype(BF16), load(i, kw + kc), preferred_element_type=F32)
            acc = o if acc is None else acc + o
        norm = jnp.sum(total, axis=-1, keepdims=True)
        att_scr[:, h * HEAD_SIZE : (h + 1) * HEAD_SIZE] = (acc / norm).astype(BF16)
    t = tp_ref[0]
    block = rows // tp_size
    for half, ref in ((0, keep_ref), (1, send_ref)):
        lhs = jnp.concatenate(
            [
                att_scr[pl.ds(pl.multiple_of((t ^ j) * block, block), block), :]
                for j in range(half, tp_size, 2)
            ],
            axis=0,
        )
        ref[...] = jnp.dot(lhs, w_ref[...], preferred_element_type=F32).astype(ref.dtype)


def pair_kernel(keep_ref, got_ref, *outs):
    first = keep_ref.shape[0] // 2
    for ref in outs:
        here = pl.ds(first, ref.shape[0])
        ref[...] = (keep_ref[here, :].astype(F32) + got_ref[here, :].astype(F32)).astype(ref.dtype)
        first += ref.shape[0]


def base_kernel(
    experts, cap, sp_ref, dep_ref, routes_ref, res_ref, gain_ref, mix_ref, down_ref, keep_ref,
    r1_ref, slot_ref, base_ref, gain_out, mix_out, down_out, routes_scr, res_scr, sem,
):
    copies = fetch(
        (
            (routes_ref, routes_scr),
            (res_ref, res_scr),
            (gain_ref, gain_out),
            (mix_ref, mix_out),
            (down_ref, down_out),
        ),
        sem,
    )
    top, rows = slot_ref.shape
    expert = lax.broadcasted_iota(jnp.int32, (experts, rows), 0)
    before = lax.broadcasted_iota(jnp.int32, (rows, rows), 0) < lax.broadcasted_iota(
        jnp.int32, (rows, rows), 1
    )
    copies[0].wait()
    marks = [(expert == routes_scr[j : j + 1, :]).astype(F32) for j in range(top)]
    earlier = jnp.dot(
        sum(marks).astype(BF16), before.astype(BF16), preferred_element_type=F32
    )
    for j in range(top):
        rank = jnp.sum(earlier * marks[j], axis=0, keepdims=True).astype(jnp.int32)
        slot_ref[j : j + 1, :] = (routes_scr[j : j + 1, :] ^ sp_ref[0]) * cap + rank
    copies[1].wait()
    base_ref[...] = (
        res_scr[...].astype(F32) + keep_ref[:rows, :].astype(F32) + r1_ref[:rows, :].astype(F32)
    )
    for c in copies[2:]:
        c.wait()


def dispatch_kernel(cap, slot_ref, gain_ref, base_ref, r2_ref, hid_ref, *outs):
    rows = base_ref.shape[0]
    hidden = base_ref[...] + r2_ref[...].astype(F32)
    hid_ref[...] = hidden
    ms = jnp.mean(hidden * hidden, axis=-1, keepdims=True)
    normed = (hidden * lax.rsqrt(ms + norm_eps) * gain_ref[...]).astype(BF16)

    def pick(first, count):
        slot = first + lax.broadcasted_iota(jnp.int32, (count, rows), 0)
        hit = slot == slot_ref[0:1, :]
        for j in range(1, slot_ref.shape[0]):
            hit = hit | (slot == slot_ref[j : j + 1, :])
        return jnp.dot(hit.astype(BF16), normed, preferred_element_type=F32).astype(BF16)

    if cap % 16 == 0:
        picked = pick(0, cap * len(outs))
        for k, ref in enumerate(outs):
            ref[...] = picked[k * cap : (k + 1) * cap, :]
    else:
        for k, ref in enumerate(outs):
            ref[...] = pick(k * cap, cap)


def join_kernel(*refs):
    parts, out_ref = refs[:-1], refs[-1]
    out_ref[...] = jnp.concatenate([r[...] for r in parts], axis=0)


def expert_kernel(nrow, fc, *refs):
    x_refs = refs[:nrow]
    g_ref, u_ref, d_ref, keep_ref, send_ref = refs[nrow:]
    x = jnp.concatenate([r[...] for r in x_refs], axis=0)
    acts = []
    for f in range(g_ref.shape[2] // fc):
        cols = slice(f * fc, (f + 1) * fc)
        gate = jnp.dot(x, g_ref[0, :, cols], preferred_element_type=F32)
        up = jnp.dot(x, u_ref[0, :, cols], preferred_element_type=F32)
        acts.append((gate / (1.0 + jnp.exp(-gate)) * up).astype(BF16))
    act = jnp.concatenate(acts, axis=1)
    half = act.shape[0] // 2
    send_ref[...] = jnp.dot(act[half:], d_ref[0], preferred_element_type=F32).astype(BF16)
    keep_ref[...] = jnp.dot(act[:half], d_ref[0], preferred_element_type=F32).astype(BF16)


def settle_kernel(first, keep_ref, r1_ref, r2_ref, *outs):
    rows = r2_ref.shape[0]
    each = rows // len(outs)
    here = pl.ds(first, rows)
    total = (
        keep_ref[here, :].astype(F32) + r1_ref[here, :].astype(F32) + r2_ref[...].astype(F32)
    ).astype(BF16)
    for k, ref in enumerate(outs):
        ref[...] = total[k * each : (k + 1) * each, :]


def combine_kernel(slot_ref, weight_ref, hid_ref, *refs):
    parts, out_ref = refs[:-1], refs[-1]
    back = jnp.concatenate([r[...] for r in parts], axis=0)
    rows = hid_ref.shape[0]
    slot = lax.broadcasted_iota(jnp.int32, (back.shape[0], rows), 0)
    same = lax.broadcasted_iota(jnp.int32, (rows, rows), 0) == lax.broadcasted_iota(
        jnp.int32, (rows, rows), 1
    )
    total = hid_ref[...]
    for j in range(slot_ref.shape[0]):
        hit = (slot == slot_ref[j : j + 1, :]).astype(BF16)
        weight = jnp.sum(jnp.where(same, weight_ref[j : j + 1, :], 0.0), axis=1, keepdims=True)
        total += weight * lax.dot_general(
            hit, back, (((0,), (0,)), ((), ())), preferred_element_type=F32
        )
    out_ref[...] = total.astype(out_ref.dtype)


def shaped(shape, dtype):
    return jax.ShapeDtypeStruct(shape, dtype)


def layer(
    queries, keys, values, query_gain, key_norm_gain, out_weight, residual, norm_gain,
    expert_gate, expert_up, expert_down, routes, route_weight,
):
    sp_size, tp_size = lax.axis_size("sp"), lax.axis_size("tp")
    sp, tp = lax.axis_index("sp"), lax.axis_index("tp")
    rows = queries.shape[0]
    qw, kw = queries.shape[1], keys.shape[1]
    heads = qw // HEAD_SIZE
    own, width = residual.shape
    route_top = routes.shape[1]
    experts = sp_size * expert_gate.shape[0]
    cap = 2 * max(1, route_top * rows // (tp_size * experts))
    sp1, tp1 = sp.astype(jnp.int32).reshape(1), tp.astype(jnp.int32).reshape(1)

    lane = shaped((rows, HEAD_SIZE), F32)
    kv, cosine, sine = call(
        key_kernel,
        (sp1, key_norm_gain.reshape(1, -1), keys, values),
        [SM, HBM, HBM, HBM],
        (VM, VM, VM),
        (shaped((rows, 2 * kw), BF16), lane, lane),
        [
            pltpu.VMEM((rows, kw), BF16),
            pltpu.VMEM((1, HEAD_SIZE), F32),
            pltpu.SemaphoreType.DMA((3,)),
        ],
    )

    half = sp_size // 2
    pieces = [kv] + [swap(kv, "sp", k) for k in range(1, sp_size)]
    if len(pieces) > 8:
        each = len(pieces) // 8
        pieces = [jnp.concatenate(pieces[i * each : (i + 1) * each], axis=0) for i in range(8)]

    q, w_near = call(
        query_kernel,
        (cosine, sine, query_gain.reshape(1, -1), queries, out_weight),
        [VM, VM, HBM, HBM, HBM],
        (VM, VM),
        (shaped((heads * rows, HEAD_SIZE), BF16), shaped(out_weight.shape, BF16)),
        [
            pltpu.VMEM((rows, qw), BF16),
            pltpu.VMEM((1, HEAD_SIZE), F32),
            pltpu.SemaphoreType.DMA((3,)),
        ],
    )

    keys_all = sum(p.shape[0] for p in pieces)
    keep, send = call(
        lambda *a: attention_kernel(len(pieces), tp_size, *a),
        (tp1, q, w_near, *pieces),
        [SM] + [VM] * (2 + len(pieces)),
        (VM, VM),
        (shaped((rows // 2, width), F32), shaped((rows // 2, width), BF16)),
        [pltpu.VMEM((rows, keys_all), F32), pltpu.VMEM((rows, qw), BF16)],
        16,
    )

    def add_pair(kept, got, splits):
        n = kept.shape[0] // (2 * splits)
        return call(
            pair_kernel, (kept, got), [VM] * 2, [VM] * splits, [shaped((n, width), BF16)] * splits
        )

    r1 = swap(send, "tp", 1)
    (pair,) = add_pair(keep, r1, 1)
    r2 = swap(pair, "tp", 2)
    slot, base, gain, mix, down = call(
        lambda *a: base_kernel(experts, cap, *a),
        (
            sp1, pair, routes.T, residual, norm_gain.reshape(1, -1), route_weight.T, expert_down,
            keep, r1,
        ),
        [SM] + [HBM] * 6 + [VM] * 2,
        (VM,) * 5,
        (
            shaped((route_top, own), jnp.int32),
            shaped((own, width), F32),
            shaped((1, width), F32),
            shaped((route_top, own), F32),
            shaped(expert_down.shape, BF16),
        ),
        [
            pltpu.VMEM((route_top, own), jnp.int32),
            pltpu.VMEM((own, width), BF16),
            pltpu.SemaphoreType.DMA((5,)),
        ],
    )

    picked = call(
        lambda *a: dispatch_kernel(cap, *a),
        (slot, gain, base, r2),
        [VM] * 4,
        [VM] * (1 + sp_size),
        [shaped((own, width), F32)] + [shaped((cap, width), BF16)] * sp_size,
    )
    hidden, mail = picked[0], picked[1:]

    inbox = [mail[0]] + [swap(mail[k], "sp", k) for k in range(1, sp_size)]
    fe = expert_gate.shape[2]
    fc = 256 if fe % 256 == 0 else fe
    returned = []
    for c in range(2):
        splits = 2 if c == 1 and half % 2 == 0 else 1
        each = half // splits
        n = cap * each
        mine = [
            call(
                join_kernel,
                inbox[c * half + i * each : c * half + (i + 1) * each],
                [VM] * each,
                VM,
                shaped((n, width), BF16),
            )
            for i in range(splits)
        ]
        core = [swap(m, "tp", 1) for m in mine]
        cross = [swap(m, "tp", 2) for m in mine]
        both = [swap(m, "tp", 1) for m in cross]
        rows_in = mine + cross + core + both
        out = shaped((2 * cap * half, width), BF16)
        keep_e, send_e = call(
            lambda *a: expert_kernel(len(rows_in), fc, *a),
            (*rows_in, expert_gate, expert_up, down),
            [VM] * (len(rows_in) + 3),
            (VM, VM),
            (out, out),
            (),
            24,
        )
        e1 = swap(send_e, "tp", 1)
        pairs = add_pair(keep_e, e1, splits)
        for i, part in enumerate(pairs):
            e2 = swap(part, "tp", 2)
            settled = call(
                functools.partial(settle_kernel, i * n),
                (keep_e, e1, e2),
                [VM] * 3,
                [VM] * each,
                [shaped((cap, width), BF16)] * each,
            )
            for k in range(each):
                peer = c * half + i * each + k
                returned.append(swap(settled[k], "sp", peer) if peer else settled[k])

    return call(
        combine_kernel,
        (slot, mix, hidden, *returned),
        [VM] * (3 + sp_size),
        VM,
        shaped((own, width), BF16),
    )


def solution(mesh):
    placed = (
        P("sp", "tp"),
        P("sp", "tp"),
        P("sp", "tp"),
        P(),
        P(),
        P("tp", None),
        P(("sp", "tp"), None),
        P(),
        P("sp", None, "tp"),
        P("sp", None, "tp"),
        P("sp", "tp", None),
        P(("sp", "tp"), None),
        P(("sp", "tp"), None),
    )
    return jax.shard_map(
        layer, mesh=mesh, in_specs=placed, out_specs=P(("sp", "tp"), None), check_vma=False
    )
```

profile of v0, /device:TPU:0, one launch (start us, length us, event | category | flops | bytes accessed | tf_op | source)
XLA Modules:
  0.0 94.7 jit_solution(17873725713901209153)
XLA Ops:
  1.0 3.1 %collective-permute-start = (bf16[128,256]{1,0:T(8,128)(2,1)S(1)}, bf16[128,256]{1,0:T(8,128)(2,1)S(1)}, u32[]{:S(2)}, u32[]{:S(2)}) collective-permute-start(bf16[128,256]{1,0:T(8,128)(2,1)S(1)} %get-tuple-element.44.a_3_), channel_id=1, source_target_pairs={{0,4},{4,0},{8,12},{12,8},{16,20},{20,16},{24,28},{28,24},{1,5},{5... | collective-permute-start | bytes 196616 | tf_op jit(solution)/shard_map/ppermute | solution.py:31
  4.1 1.6 %collective-permute-start.1 = (bf16[128,256]{1,0:T(8,128)(2,1)S(1)}, bf16[128,256]{1,0:T(8,128)(2,1)S(1)}, u32[]{:S(2)}, u32[]{:S(2)}) collective-permute-start(bf16[128,256]{1,0:T(8,128)(2,1)S(1)} %get-tuple-element.44.a_3_), channel_id=1, source_target_pairs={{0,8},{4,12},{8,0},{12,4},{16,24},{20,28},{24,16},{28,20},{1,9},{5... | collective-permute-start | bytes 196616 | tf_op jit(solution)/shard_map/ppermute | solution.py:31
  5.6 3.0 %collective-permute-start.3 = (bf16[128,256]{1,0:T(8,128)(2,1)S(1)}, bf16[128,256]{1,0:T(8,128)(2,1)S(1)}, u32[]{:S(2)}, u32[]{:S(2)}) collective-permute-start(bf16[128,256]{1,0:T(8,128)(2,1)S(1)} %get-tuple-element.44.a_3_), channel_id=1, source_target_pairs={{0,16},{4,20},{8,24},{12,28},{16,0},{20,4},{24,8},{28,12},{1,17},{... | collective-permute-start | bytes 196616 | tf_op jit(solution)/shard_map/ppermute | solution.py:31
  8.6 1.3 %collective-permute-start.4 = (bf16[128,256]{1,0:T(8,128)(2,1)S(1)}, bf16[128,256]{1,0:T(8,128)(2,1)S(1)}, u32[]{:S(2)}, u32[]{:S(2)}) collective-permute-start(bf16[128,256]{1,0:T(8,128)(2,1)S(1)} %get-tuple-element.44.a_3_), channel_id=1, source_target_pairs={{0,20},{4,16},{8,28},{12,24},{16,4},{20,0},{24,12},{28,8},{1,21},{... | collective-permute-start | bytes 196616 | tf_op jit(solution)/shard_map/ppermute | solution.py:31
  9.9 3.6 %collective-permute-start.5 = (bf16[128,256]{1,0:T(8,128)(2,1)S(1)}, bf16[128,256]{1,0:T(8,128)(2,1)S(1)}, u32[]{:S(2)}, u32[]{:S(2)}) collective-permute-start(bf16[128,256]{1,0:T(8,128)(2,1)S(1)} %get-tuple-element.44.a_3_), channel_id=1, source_target_pairs={{0,24},{4,28},{8,16},{12,20},{16,8},{20,12},{24,0},{28,4},{1,25},{... | collective-permute-start | bytes 196616 | tf_op jit(solution)/shard_map/ppermute | solution.py:31
  13.5 1.7 %shard_map.128 = (bf16[512,128]{1,0:T(8,128)(2,1)S(1)}, bf16[512,2048]{1,0:T(8,128)(2,1)S(1)}) custom-call(f32[128,128]{1,0:T(8,128)S(1)} %get-tuple-element.40.cos_ref, f32[128,128]{1,0:T(8,128)S(1)} %get-tuple-element.41.sin_ref, f32[1,128]{1,0:T(1,128)} %bitcast.11, bf16[128,512]{1,0:T(8,128)(2,1)} %q_ref.1, bf16[512,2048]{1,0:T(8,128)(2,1)} %w_ref.1), custom_call_target="tpu_custom_call" | custom-call | tf_op jit(solution)/shard_map/pallas_call | solution.py:39
  15.3 3.6 %collective-permute-done.4.a_8_ = bf16[128,256]{1,0:T(8,128)(2,1)S(1)} collective-permute-done((bf16[128,256]{1,0:T(8,128)(2,1)S(1)}, bf16[128,256]{1,0:T(8,128)(2,1)S(1)}, u32[]{:S(2)}, u32[]{:S(2)}) %collective-permute-start.4) | collective-permute-done | bytes 65568 | tf_op jit(solution)/shard_map/ppermute | solution.py:31
  18.8 1.8 %collective-permute-done.6.a_10_ = bf16[128,256]{1,0:T(8,128)(2,1)S(1)} collective-permute-done((bf16[128,256]{1,0:T(8,128)(2,1)S(1)}, bf16[128,256]{1,0:T(8,128)(2,1)S(1)}, u32[]{:S(2)}, u32[]{:S(2)}) %collective-permute-start.6) | collective-permute-done | bytes 65568 | tf_op jit(solution)/shard_map/ppermute | solution.py:31
  20.6 2.4 %shard_map.129 = (f32[64,2048]{1,0:T(8,128)S(1)}, bf16[64,2048]{1,0:T(8,128)(2,1)S(1)}) custom-call(s32[1]{0:T(128)} %bitcast.1.a_0_, bf16[512,128]{1,0:T(8,128)(2,1)S(1)} %get-tuple-element.42.a_1_, bf16[512,2048]{1,0:T(8,128)(2,1)S(1)} %get-tuple-element.43.a_2_, bf16[128,256]{1,0:T(8,128)(2,1)S(1)} %get-tuple-element.44.a_3_, ...), custom_call_target="tpu_custom_call" | custom-call | tf_op jit(solution)/shard_map/pallas_call | solution.py:39
  23.0 1.5 %collective-permute-done.7.got_ref.a_8_ = bf16[64,2048]{1,0:T(8,128)(2,1)S(1)} collective-permute-done((bf16[64,2048]{1,0:T(8,128)(2,1)S(1)}, bf16[64,2048]{1,0:T(8,128)(2,1)S(1)}, u32[]{:S(2)}, u32[]{:S(2)}) %collective-permute-start.7) | collective-permute-done | bytes 262176 | tf_op jit(solution)/shard_map/ppermute | solution.py:31
  24.6 1.6 %collective-permute-start.8 = (bf16[32,2048]{1,0:T(8,128)(2,1)S(1)}, bf16[32,2048]{1,0:T(8,128)(2,1)S(1)}, u32[]{:S(2)}, u32[]{:S(2)}) collective-permute-start(bf16[32,2048]{1,0:T(8,128)(2,1)S(1)} %shard_map.130.a_1_), channel_id=1, source_target_pairs={{0,2},{1,3},{2,0},{3,1},{4,6},{5,7},{6,4},{7,5},{8,10},{9,11},{10,... | collective-permute-start | bytes 393224 | tf_op jit(solution)/shard_map/ppermute | solution.py:31
  26.2 2.3 %shard_map.131 = (s32[2,32]{1,0:T(2,128)S(1)}, f32[32,2048]{1,0:T(8,128)S(1)}, f32[1,2048]{1,0:T(1,128)S(1)}, f32[2,32]{1,0:T(2,128)S(1)}, bf16[1,768,2048]{2,1,0:T(8,128)(2,1)S(1)}) custom-call(s32[1]{0:T(128)} %bitcast.sp_ref.a_0_, bf16[32,2048]{1,0:T(8,128)(2,1)} %copy-done.2, s32[2,32]{1,0:T(2,128)} %bitcast.8, bf16[32,2048]{1,0:T(8,128)(2,1)} %a_3_.1, ...), custom_call_target="tpu_custom_call" | custom-call | tf_op jit(solution)/shard_map/pallas_call | solution.py:39
  28.5 1.7 %collective-permute-done.8.a_3_ = bf16[32,2048]{1,0:T(8,128)(2,1)S(1)} collective-permute-done((bf16[32,2048]{1,0:T(8,128)(2,1)S(1)}, bf16[32,2048]{1,0:T(8,128)(2,1)S(1)}, u32[]{:S(2)}, u32[]{:S(2)}) %collective-permute-start.8) | collective-permute-done | bytes 131104 | tf_op jit(solution)/shard_map/ppermute | solution.py:31
  31.2 2.0 %collective-permute-start.10 = (bf16[16,2048]{1,0:T(8,128)(2,1)S(1)}, bf16[16,2048]{1,0:T(8,128)(2,1)S(1)}, u32[]{:S(2)}, u32[]{:S(2)}) collective-permute-start(bf16[16,2048]{1,0:T(8,128)(2,1)S(1)} %get-tuple-element.54), channel_id=1, source_target_pairs={{0,8},{4,12},{8,0},{12,4},{16,24},{20,28},{24,16},{28,20},{1,9},{5... | collective-permute-start | bytes 196616 | tf_op jit(solution)/shard_map/ppermute | solution.py:31
  35.8 2.5 %collective-permute-done.11.refs_3_ = bf16[16,2048]{1,0:T(8,128)(2,1)S(1)} collective-permute-done((bf16[16,2048]{1,0:T(8,128)(2,1)S(1)}, bf16[16,2048]{1,0:T(8,128)(2,1)S(1)}, u32[]{:S(2)}, u32[]{:S(2)}) %collective-permute-start.11) | collective-permute-done | bytes 65568 | tf_op jit(solution)/shard_map/ppermute | solution.py:31
  38.3 1.6 %collective-permute-start.12 = (bf16[64,2048]{1,0:T(8,128)(2,1)S(1)}, bf16[64,2048]{1,0:T(8,128)(2,1)S(1)}, u32[]{:S(2)}, u32[]{:S(2)}) collective-permute-start(bf16[64,2048]{1,0:T(8,128)(2,1)S(1)} %shard_map.133.a_0_), channel_id=1, source_target_pairs={{0,2},{1,3},{2,0},{3,1},{4,6},{5,7},{6,4},{7,5},{8,10},{9,11},{10,... | collective-permute-start | bytes 786440 | tf_op jit(solution)/shard_map/ppermute | solution.py:31
  39.9 1.6 %collective-permute-start.20 = (bf16[16,2048]{1,0:T(8,128)(2,1)S(1)}, bf16[16,2048]{1,0:T(8,128)(2,1)S(1)}, u32[]{:S(2)}, u32[]{:S(2)}) collective-permute-start(bf16[16,2048]{1,0:T(8,128)(2,1)S(1)} %get-tuple-element.63), channel_id=1, source_target_pairs={{0,16},{4,20},{8,24},{12,28},{16,0},{20,4},{24,8},{28,12},{1,17},{... | collective-permute-start | bytes 196616 | tf_op jit(solution)/shard_map/ppermute | solution.py:31
  41.5 2.0 %collective-permute-start.21 = (bf16[16,2048]{1,0:T(8,128)(2,1)S(1)}, bf16[16,2048]{1,0:T(8,128)(2,1)S(1)}, u32[]{:S(2)}, u32[]{:S(2)}) collective-permute-start(bf16[16,2048]{1,0:T(8,128)(2,1)S(1)} %get-tuple-element.64), channel_id=1, source_target_pairs={{0,20},{4,16},{8,28},{12,24},{16,4},{20,0},{24,12},{28,8},{1,21},{... | collective-permute-start | bytes 196616 | tf_op jit(solution)/shard_map/ppermute | solution.py:31
  43.5 2.6 %collective-permute-start.22 = (bf16[16,2048]{1,0:T(8,128)(2,1)S(1)}, bf16[16,2048]{1,0:T(8,128)(2,1)S(1)}, u32[]{:S(2)}, u32[]{:S(2)}) collective-permute-start(bf16[16,2048]{1,0:T(8,128)(2,1)S(1)} %get-tuple-element.65), channel_id=1, source_target_pairs={{0,24},{4,28},{8,16},{12,20},{16,8},{20,12},{24,0},{28,4},{1,25},{... | collective-permute-start | bytes 196616 | tf_op jit(solution)/shard_map/ppermute | solution.py:31
  46.1 4.5 %collective-permute-start.23 = (bf16[16,2048]{1,0:T(8,128)(2,1)S(1)}, bf16[16,2048]{1,0:T(8,128)(2,1)S(1)}, u32[]{:S(2)}, u32[]{:S(2)}) collective-permute-start(bf16[16,2048]{1,0:T(8,128)(2,1)S(1)} %get-tuple-element.66), channel_id=1, source_target_pairs={{0,28},{4,24},{8,20},{12,16},{16,12},{20,8},{24,4},{28,0},{1,29},{... | collective-permute-start | bytes 196616 | tf_op jit(solution)/shard_map/ppermute | solution.py:31
  51.7 1.4 %collective-permute-done.23.refs_1_ = bf16[16,2048]{1,0:T(8,128)(2,1)S(1)} collective-permute-done((bf16[16,2048]{1,0:T(8,128)(2,1)S(1)}, bf16[16,2048]{1,0:T(8,128)(2,1)S(1)}, u32[]{:S(2)}, u32[]{:S(2)}) %collective-permute-start.23) | collective-permute-done | bytes 65568 | tf_op jit(solution)/shard_map/ppermute | solution.py:31
  53.6 3.9 %collective-permute-done.24.a_2_ = bf16[32,2048]{1,0:T(8,128)(2,1)S(1)} collective-permute-done((bf16[32,2048]{1,0:T(8,128)(2,1)S(1)}, bf16[32,2048]{1,0:T(8,128)(2,1)S(1)}, u32[]{:S(2)}, u32[]{:S(2)}) %collective-permute-start.24) | collective-permute-done | bytes 131104 | tf_op jit(solution)/shard_map/ppermute | solution.py:31
  57.5 1.8 %collective-permute-done.25.a_3_ = bf16[32,2048]{1,0:T(8,128)(2,1)S(1)} collective-permute-done((bf16[32,2048]{1,0:T(8,128)(2,1)S(1)}, bf16[32,2048]{1,0:T(8,128)(2,1)S(1)}, u32[]{:S(2)}, u32[]{:S(2)}) %collective-permute-start.25) | collective-permute-done | bytes 131104 | tf_op jit(solution)/shard_map/ppermute | solution.py:31
  59.9 2.7 %shard_map.134 = (bf16[128,2048]{1,0:T(8,128)(2,1)S(1)}, bf16[128,2048]{1,0:T(8,128)(2,1)S(1)}) custom-call(bf16[64,2048]{1,0:T(8,128)(2,1)S(1)} %shard_map.133.a_0_, bf16[64,2048]{1,0:T(8,128)(2,1)S(1)} %collective-permute-done.12.a_1_, bf16[64,2048]{1,0:T(8,128)(2,1)S(1)} %collective-permute-done.13.a_2_, ...), custom_call_target="tpu_custom_call" | custom-call | tf_op jit(solution)/shard_map/pallas_call | solution.py:39
  62.7 2.7 %shard_map.139 = (bf16[128,2048]{1,0:T(8,128)(2,1)S(1)}, bf16[128,2048]{1,0:T(8,128)(2,1)S(1)}) custom-call(bf16[32,2048]{1,0:T(8,128)(2,1)S(1)} %shard_map.137.a_0_, bf16[32,2048]{1,0:T(8,128)(2,1)S(1)} %shard_map.138.a_1_, bf16[32,2048]{1,0:T(8,128)(2,1)S(1)} %collective-permute-done.24.a_2_, bf16[32,2048]{1,0:T(8,128)(2,1)S(1)} %collective-permute-done.25.a_3_, ...), custom_call_target="tpu_custom_call" | custom-call | tf_op jit(solution)/shard_map/pallas_call | solution.py:39
  68.2 1.4 %collective-permute-start.34 = (bf16[32,2048]{1,0:T(8,128)(2,1)S(1)}, bf16[32,2048]{1,0:T(8,128)(2,1)S(1)}, u32[]{:S(2)}, u32[]{:S(2)}) collective-permute-start(bf16[32,2048]{1,0:T(8,128)(2,1)S(1)} %get-tuple-element.72), channel_id=1, source_target_pairs={{0,2},{1,3},{2,0},{3,1},{4,6},{5,7},{6,4},{7,5},{8,10},{9,11},{10,... | collective-permute-start | bytes 393224 | tf_op jit(solution)/shard_map/ppermute | solution.py:31
  69.6 8.4 %collective-permute-done.31.r2_ref = bf16[32,2048]{1,0:T(8,128)(2,1)S(1)} collective-permute-done((bf16[32,2048]{1,0:T(8,128)(2,1)S(1)}, bf16[32,2048]{1,0:T(8,128)(2,1)S(1)}, u32[]{:S(2)}, u32[]{:S(2)}) %collective-permute-start.31) | collective-permute-done | bytes 131104 | tf_op jit(solution)/shard_map/ppermute | solution.py:31
  78.1 1.7 %collective-permute-start.32 = (bf16[16,2048]{1,0:T(8,128)(2,1)S(1)}, bf16[16,2048]{1,0:T(8,128)(2,1)S(1)}, u32[]{:S(2)}, u32[]{:S(2)}) collective-permute-start(bf16[16,2048]{1,0:T(8,128)(2,1)S(1)} %get-tuple-element.70), channel_id=1, source_target_pairs={{0,16},{4,20},{8,24},{12,28},{16,0},{20,4},{24,8},{28,12},{1,17},{... | collective-permute-start | bytes 196616 | tf_op jit(solution)/shard_map/ppermute | solution.py:31
  80.5 4.0 %collective-permute-start.35 = (bf16[16,2048]{1,0:T(8,128)(2,1)S(1)}, bf16[16,2048]{1,0:T(8,128)(2,1)S(1)}, u32[]{:S(2)}, u32[]{:S(2)}) collective-permute-start(bf16[16,2048]{1,0:T(8,128)(2,1)S(1)} %get-tuple-element.73), channel_id=1, source_target_pairs={{0,24},{4,28},{8,16},{12,20},{16,8},{20,12},{24,0},{28,4},{1,25},{... | collective-permute-start | bytes 196616 | tf_op jit(solution)/shard_map/ppermute | solution.py:31
  84.4 1.5 %collective-permute-start.36 = (bf16[16,2048]{1,0:T(8,128)(2,1)S(1)}, bf16[16,2048]{1,0:T(8,128)(2,1)S(1)}, u32[]{:S(2)}, u32[]{:S(2)}) collective-permute-start(bf16[16,2048]{1,0:T(8,128)(2,1)S(1)} %get-tuple-element.74), channel_id=1, source_target_pairs={{0,28},{4,24},{8,20},{12,16},{16,12},{20,8},{24,4},{28,0},{1,29},{... | collective-permute-start | bytes 196616 | tf_op jit(solution)/shard_map/ppermute | solution.py:31
  86.1 2.2 %collective-permute-done.32.refs_4_ = bf16[16,2048]{1,0:T(8,128)(2,1)S(1)} collective-permute-done((bf16[16,2048]{1,0:T(8,128)(2,1)S(1)}, bf16[16,2048]{1,0:T(8,128)(2,1)S(1)}, u32[]{:S(2)}, u32[]{:S(2)}) %collective-permute-start.32) | collective-permute-done | bytes 65568 | tf_op jit(solution)/shard_map/ppermute | solution.py:31
  89.6 1.9 %collective-permute-done.36.refs_7_ = bf16[16,2048]{1,0:T(8,128)(2,1)S(1)} collective-permute-done((bf16[16,2048]{1,0:T(8,128)(2,1)S(1)}, bf16[16,2048]{1,0:T(8,128)(2,1)S(1)}, u32[]{:S(2)}, u32[]{:S(2)}) %collective-permute-start.36) | collective-permute-done | bytes 65568 | tf_op jit(solution)/shard_map/ppermute | solution.py:31
  (65 shorter events, 15.3 us)
Async XLA Ops:
  1.0 8.9 %collective-permute-start = (bf16[128,256]{1,0:T(8,128)(2,1)S(1)}, bf16[128,256]{1,0:T(8,128)(2,1)S(1)}, u32[]{:S(2)}, u32[]{:S(2)}) collective-permute-start(bf16[128,256]{1,0:T(8,128)(2,1)S(1)} %get-tuple-element.44.a_3_), channel_id=1, source_target_pairs={{0,4},{4,0},{8,12},{12,8},{16,20},{20,16},{24,28},{28,24},{1,5},{5... | collective-permute-start | bytes 196616 | tf_op jit(solution)/shard_map/ppermute | solution.py:31
  4.1 9.5 %collective-permute-start.1 = (bf16[128,256]{1,0:T(8,128)(2,1)S(1)}, bf16[128,256]{1,0:T(8,128)(2,1)S(1)}, u32[]{:S(2)}, u32[]{:S(2)}) collective-permute-start(bf16[128,256]{1,0:T(8,128)(2,1)S(1)} %get-tuple-element.44.a_3_), channel_id=1, source_target_pairs={{0,8},{4,12},{8,0},{12,4},{16,24},{20,28},{24,16},{28,20},{1,9},{5... | collective-permute-start | bytes 196616 | tf_op jit(solution)/shard_map/ppermute | solution.py:31
  5.6 9.6 %collective-permute-start.2 = (bf16[128,256]{1,0:T(8,128)(2,1)S(1)}, bf16[128,256]{1,0:T(8,128)(2,1)S(1)}, u32[]{:S(2)}, u32[]{:S(2)}) collective-permute-start(bf16[128,256]{1,0:T(8,128)(2,1)S(1)} %get-tuple-element.44.a_3_), channel_id=1, source_target_pairs={{0,12},{4,8},{8,4},{12,0},{16,28},{20,24},{24,20},{28,16},{1,13},{... | collective-permute-start | bytes 196616 | tf_op jit(solution)/shard_map/ppermute | solution.py:31
  5.6 9.6 %collective-permute-start.3 = (bf16[128,256]{1,0:T(8,128)(2,1)S(1)}, bf16[128,256]{1,0:T(8,128)(2,1)S(1)}, u32[]{:S(2)}, u32[]{:S(2)}) collective-permute-start(bf16[128,256]{1,0:T(8,128)(2,1)S(1)} %get-tuple-element.44.a_3_), channel_id=1, source_target_pairs={{0,16},{4,20},{8,24},{12,28},{16,0},{20,4},{24,8},{28,12},{1,17},{... | collective-permute-start | bytes 196616 | tf_op jit(solution)/shard_map/ppermute | solution.py:31
  8.6 10.2 %collective-permute-start.4 = (bf16[128,256]{1,0:T(8,128)(2,1)S(1)}, bf16[128,256]{1,0:T(8,128)(2,1)S(1)}, u32[]{:S(2)}, u32[]{:S(2)}) collective-permute-start(bf16[128,256]{1,0:T(8,128)(2,1)S(1)} %get-tuple-element.44.a_3_), channel_id=1, source_target_pairs={{0,20},{4,16},{8,28},{12,24},{16,4},{20,0},{24,12},{28,8},{1,21},{... | collective-permute-start | bytes 196616 | tf_op jit(solution)/shard_map/ppermute | solution.py:31
  9.9 8.9 %collective-permute-start.5 = (bf16[128,256]{1,0:T(8,128)(2,1)S(1)}, bf16[128,256]{1,0:T(8,128)(2,1)S(1)}, u32[]{:S(2)}, u32[]{:S(2)}) collective-permute-start(bf16[128,256]{1,0:T(8,128)(2,1)S(1)} %get-tuple-element.44.a_3_), channel_id=1, source_target_pairs={{0,24},{4,28},{8,16},{12,20},{16,8},{20,12},{24,0},{28,4},{1,25},{... | collective-permute-start | bytes 196616 | tf_op jit(solution)/shard_map/ppermute | solution.py:31
  13.5 7.1 %collective-permute-start.6 = (bf16[128,256]{1,0:T(8,128)(2,1)S(1)}, bf16[128,256]{1,0:T(8,128)(2,1)S(1)}, u32[]{:S(2)}, u32[]{:S(2)}) collective-permute-start(bf16[128,256]{1,0:T(8,128)(2,1)S(1)} %get-tuple-element.44.a_3_), channel_id=1, source_target_pairs={{0,28},{4,24},{8,20},{12,16},{16,12},{20,8},{24,4},{28,0},{1,29},{... | collective-permute-start | bytes 196616 | tf_op jit(solution)/shard_map/ppermute | solution.py:31
  24.6 5.6 %collective-permute-start.8 = (bf16[32,2048]{1,0:T(8,128)(2,1)S(1)}, bf16[32,2048]{1,0:T(8,128)(2,1)S(1)}, u32[]{:S(2)}, u32[]{:S(2)}) collective-permute-start(bf16[32,2048]{1,0:T(8,128)(2,1)S(1)} %shard_map.130.a_1_), channel_id=1, source_target_pairs={{0,2},{1,3},{2,0},{3,1},{4,6},{5,7},{6,4},{7,5},{8,10},{9,11},{10,... | collective-permute-start | bytes 393224 | tf_op jit(solution)/shard_map/ppermute | solution.py:31
  30.6 4.3 %collective-permute-start.9 = (bf16[16,2048]{1,0:T(8,128)(2,1)S(1)}, bf16[16,2048]{1,0:T(8,128)(2,1)S(1)}, u32[]{:S(2)}, u32[]{:S(2)}) collective-permute-start(bf16[16,2048]{1,0:T(8,128)(2,1)S(1)} %get-tuple-element.53), channel_id=1, source_target_pairs={{0,4},{4,0},{8,12},{12,8},{16,20},{20,16},{24,28},{28,24},{1,5},{5... | collective-permute-start | bytes 196616 | tf_op jit(solution)/shard_map/ppermute | solution.py:31
  31.2 4.6 %collective-permute-start.10 = (bf16[16,2048]{1,0:T(8,128)(2,1)S(1)}, bf16[16,2048]{1,0:T(8,128)(2,1)S(1)}, u32[]{:S(2)}, u32[]{:S(2)}) collective-permute-start(bf16[16,2048]{1,0:T(8,128)(2,1)S(1)} %get-tuple-element.54), channel_id=1, source_target_pairs={{0,8},{4,12},{8,0},{12,4},{16,24},{20,28},{24,16},{28,20},{1,9},{5... | collective-permute-start | bytes 196616 | tf_op jit(solution)/shard_map/ppermute | solution.py:31
  33.1 5.2 %collective-permute-start.11 = (bf16[16,2048]{1,0:T(8,128)(2,1)S(1)}, bf16[16,2048]{1,0:T(8,128)(2,1)S(1)}, u32[]{:S(2)}, u32[]{:S(2)}) collective-permute-start(bf16[16,2048]{1,0:T(8,128)(2,1)S(1)} %get-tuple-element.55), channel_id=1, source_target_pairs={{0,12},{4,8},{8,4},{12,0},{16,28},{20,24},{24,20},{28,16},{1,13},{... | collective-permute-start | bytes 196616 | tf_op jit(solution)/shard_map/ppermute | solution.py:31
  38.3 12.2 %collective-permute-start.12 = (bf16[64,2048]{1,0:T(8,128)(2,1)S(1)}, bf16[64,2048]{1,0:T(8,128)(2,1)S(1)}, u32[]{:S(2)}, u32[]{:S(2)}) collective-permute-start(bf16[64,2048]{1,0:T(8,128)(2,1)S(1)} %shard_map.133.a_0_), channel_id=1, source_target_pairs={{0,2},{1,3},{2,0},{3,1},{4,6},{5,7},{6,4},{7,5},{8,10},{9,11},{10,... | collective-permute-start | bytes 786440 | tf_op jit(solution)/shard_map/ppermute | solution.py:31
  39.9 6.2 %collective-permute-start.20 = (bf16[16,2048]{1,0:T(8,128)(2,1)S(1)}, bf16[16,2048]{1,0:T(8,128)(2,1)S(1)}, u32[]{:S(2)}, u32[]{:S(2)}) collective-permute-start(bf16[16,2048]{1,0:T(8,128)(2,1)S(1)} %get-tuple-element.63), channel_id=1, source_target_pairs={{0,16},{4,20},{8,24},{12,28},{16,0},{20,4},{24,8},{28,12},{1,17},{... | collective-permute-start | bytes 196616 | tf_op jit(solution)/shard_map/ppermute | solution.py:31
  41.5 17.9 %collective-permute-start.13 = (bf16[64,2048]{1,0:T(8,128)(2,1)S(1)}, bf16[64,2048]{1,0:T(8,128)(2,1)S(1)}, u32[]{:S(2)}, u32[]{:S(2)}) collective-permute-start(bf16[64,2048]{1,0:T(8,128)(2,1)S(1)} %shard_map.133.a_0_), channel_id=1, source_target_pairs={{0,1},{1,0},{2,3},{3,2},{4,5},{5,4},{6,7},{7,6},{8,9},{9,8},{10,11... | collective-permute-start | bytes 786440 | tf_op jit(solution)/shard_map/ppermute | solution.py:31
  41.5 9.6 %collective-permute-start.21 = (bf16[16,2048]{1,0:T(8,128)(2,1)S(1)}, bf16[16,2048]{1,0:T(8,128)(2,1)S(1)}, u32[]{:S(2)}, u32[]{:S(2)}) collective-permute-start(bf16[16,2048]{1,0:T(8,128)(2,1)S(1)} %get-tuple-element.64), channel_id=1, source_target_pairs={{0,20},{4,16},{8,28},{12,24},{16,4},{20,0},{24,12},{28,8},{1,21},{... | collective-permute-start | bytes 196616 | tf_op jit(solution)/shard_map/ppermute | solution.py:31
  43.5 8.2 %collective-permute-start.22 = (bf16[16,2048]{1,0:T(8,128)(2,1)S(1)}, bf16[16,2048]{1,0:T(8,128)(2,1)S(1)}, u32[]{:S(2)}, u32[]{:S(2)}) collective-permute-start(bf16[16,2048]{1,0:T(8,128)(2,1)S(1)} %get-tuple-element.65), channel_id=1, source_target_pairs={{0,24},{4,28},{8,16},{12,20},{16,8},{20,12},{24,0},{28,4},{1,25},{... | collective-permute-start | bytes 196616 | tf_op jit(solution)/shard_map/ppermute | solution.py:31
  46.1 7.0 %collective-permute-start.23 = (bf16[16,2048]{1,0:T(8,128)(2,1)S(1)}, bf16[16,2048]{1,0:T(8,128)(2,1)S(1)}, u32[]{:S(2)}, u32[]{:S(2)}) collective-permute-start(bf16[16,2048]{1,0:T(8,128)(2,1)S(1)} %get-tuple-element.66), channel_id=1, source_target_pairs={{0,28},{4,24},{8,20},{12,16},{16,12},{20,8},{24,4},{28,0},{1,29},{... | collective-permute-start | bytes 196616 | tf_op jit(solution)/shard_map/ppermute | solution.py:31
  50.5 9.3 %collective-permute-start.14 = (bf16[64,2048]{1,0:T(8,128)(2,1)S(1)}, bf16[64,2048]{1,0:T(8,128)(2,1)S(1)}, u32[]{:S(2)}, u32[]{:S(2)}) collective-permute-start(bf16[64,2048]{1,0:T(8,128)(2,1)S(1)} %collective-permute-done.12.a_1_), channel_id=1, source_target_pairs={{0,1},{1,0},{2,3},{3,2},{4,5},{5,4},{6,7},{7,6},{8,9},{9,8},{10,11... | collective-permute-start | bytes 786440 | tf_op jit(solution)/shard_map/ppermute | solution.py:31
  51.1 6.4 %collective-permute-start.24 = (bf16[32,2048]{1,0:T(8,128)(2,1)S(1)}, bf16[32,2048]{1,0:T(8,128)(2,1)S(1)}, u32[]{:S(2)}, u32[]{:S(2)}) collective-permute-start(bf16[32,2048]{1,0:T(8,128)(2,1)S(1)} %shard_map.137.a_0_), channel_id=1, source_target_pairs={{0,2},{1,3},{2,0},{3,1},{4,6},{5,7},{6,4},{7,5},{8,10},{9,11},{10,... | collective-permute-start | bytes 393224 | tf_op jit(solution)/shard_map/ppermute | solution.py:31
  53.0 6.3 %collective-permute-start.25 = (bf16[32,2048]{1,0:T(8,128)(2,1)S(1)}, bf16[32,2048]{1,0:T(8,128)(2,1)S(1)}, u32[]{:S(2)}, u32[]{:S(2)}) collective-permute-start(bf16[32,2048]{1,0:T(8,128)(2,1)S(1)} %shard_map.138.a_1_), channel_id=1, source_target_pairs={{0,2},{1,3},{2,0},{3,1},{4,6},{5,7},{6,4},{7,5},{8,10},{9,11},{10,... | collective-permute-start | bytes 393224 | tf_op jit(solution)/shard_map/ppermute | solution.py:31
  53.6 9.0 %collective-permute-start.26 = (bf16[32,2048]{1,0:T(8,128)(2,1)S(1)}, bf16[32,2048]{1,0:T(8,128)(2,1)S(1)}, u32[]{:S(2)}, u32[]{:S(2)}) collective-permute-start(bf16[32,2048]{1,0:T(8,128)(2,1)S(1)} %shard_map.137.a_0_), channel_id=1, source_target_pairs={{0,1},{1,0},{2,3},{3,2},{4,5},{5,4},{6,7},{7,6},{8,9},{9,8},{10,11... | collective-permute-start | bytes 393224 | tf_op jit(solution)/shard_map/ppermute | solution.py:31
  57.5 5.2 %collective-permute-start.27 = (bf16[32,2048]{1,0:T(8,128)(2,1)S(1)}, bf16[32,2048]{1,0:T(8,128)(2,1)S(1)}, u32[]{:S(2)}, u32[]{:S(2)}) collective-permute-start(bf16[32,2048]{1,0:T(8,128)(2,1)S(1)} %shard_map.138.a_1_), channel_id=1, source_target_pairs={{0,1},{1,0},{2,3},{3,2},{4,5},{5,4},{6,7},{7,6},{8,9},{9,8},{10,11... | collective-permute-start | bytes 393224 | tf_op jit(solution)/shard_map/ppermute | solution.py:31
  66.0 19.9 %collective-permute-start.16 = (bf16[64,2048]{1,0:T(8,128)(2,1)S(1)}, bf16[64,2048]{1,0:T(8,128)(2,1)S(1)}, u32[]{:S(2)}, u32[]{:S(2)}) collective-permute-start(bf16[64,2048]{1,0:T(8,128)(2,1)S(1)} %shard_map.135), channel_id=1, source_target_pairs={{0,2},{1,3},{2,0},{3,1},{4,6},{5,7},{6,4},{7,5},{8,10},{9,11},{10,... | collective-permute-start | bytes 786440 | tf_op jit(solution)/shard_map/ppermute | solution.py:31
  67.5 10.5 %collective-permute-start.31 = (bf16[32,2048]{1,0:T(8,128)(2,1)S(1)}, bf16[32,2048]{1,0:T(8,128)(2,1)S(1)}, u32[]{:S(2)}, u32[]{:S(2)}) collective-permute-start(bf16[32,2048]{1,0:T(8,128)(2,1)S(1)} %get-tuple-element.69), channel_id=1, source_target_pairs={{0,2},{1,3},{2,0},{3,1},{4,6},{5,7},{6,4},{7,5},{8,10},{9,11},{10,... | collective-permute-start | bytes 393224 | tf_op jit(solution)/shard_map/ppermute | solution.py:31
  68.2 12.2 %collective-permute-start.34 = (bf16[32,2048]{1,0:T(8,128)(2,1)S(1)}, bf16[32,2048]{1,0:T(8,128)(2,1)S(1)}, u32[]{:S(2)}, u32[]{:S(2)}) collective-permute-start(bf16[32,2048]{1,0:T(8,128)(2,1)S(1)} %get-tuple-element.72), channel_id=1, source_target_pairs={{0,2},{1,3},{2,0},{3,1},{4,6},{5,7},{6,4},{7,5},{8,10},{9,11},{10,... | collective-permute-start | bytes 393224 | tf_op jit(solution)/shard_map/ppermute | solution.py:31
  78.1 10.2 %collective-permute-start.32 = (bf16[16,2048]{1,0:T(8,128)(2,1)S(1)}, bf16[16,2048]{1,0:T(8,128)(2,1)S(1)}, u32[]{:S(2)}, u32[]{:S(2)}) collective-permute-start(bf16[16,2048]{1,0:T(8,128)(2,1)S(1)} %get-tuple-element.70), channel_id=1, source_target_pairs={{0,16},{4,20},{8,24},{12,28},{16,0},{20,4},{24,8},{28,12},{1,17},{... | collective-permute-start | bytes 196616 | tf_op jit(solution)/shard_map/ppermute | solution.py:31
  79.8 8.7 %collective-permute-start.33 = (bf16[16,2048]{1,0:T(8,128)(2,1)S(1)}, bf16[16,2048]{1,0:T(8,128)(2,1)S(1)}, u32[]{:S(2)}, u32[]{:S(2)}) collective-permute-start(bf16[16,2048]{1,0:T(8,128)(2,1)S(1)} %get-tuple-element.71), channel_id=1, source_target_pairs={{0,20},{4,16},{8,28},{12,24},{16,4},{20,0},{24,12},{28,8},{1,21},{... | collective-permute-start | bytes 196616 | tf_op jit(solution)/shard_map/ppermute | solution.py:31
  80.5 9.1 %collective-permute-start.35 = (bf16[16,2048]{1,0:T(8,128)(2,1)S(1)}, bf16[16,2048]{1,0:T(8,128)(2,1)S(1)}, u32[]{:S(2)}, u32[]{:S(2)}) collective-permute-start(bf16[16,2048]{1,0:T(8,128)(2,1)S(1)} %get-tuple-element.73), channel_id=1, source_target_pairs={{0,24},{4,28},{8,16},{12,20},{16,8},{20,12},{24,0},{28,4},{1,25},{... | collective-permute-start | bytes 196616 | tf_op jit(solution)/shard_map/ppermute | solution.py:31
  84.4 7.1 %collective-permute-start.36 = (bf16[16,2048]{1,0:T(8,128)(2,1)S(1)}, bf16[16,2048]{1,0:T(8,128)(2,1)S(1)}, u32[]{:S(2)}, u32[]{:S(2)}) collective-permute-start(bf16[16,2048]{1,0:T(8,128)(2,1)S(1)} %get-tuple-element.74), channel_id=1, source_target_pairs={{0,28},{4,24},{8,20},{12,16},{16,12},{20,8},{24,4},{28,0},{1,29},{... | collective-permute-start | bytes 196616 | tf_op jit(solution)/shard_map/ppermute | solution.py:31
  86.1 5.6 %collective-permute-start.17 = (bf16[16,2048]{1,0:T(8,128)(2,1)S(1)}, bf16[16,2048]{1,0:T(8,128)(2,1)S(1)}, u32[]{:S(2)}, u32[]{:S(2)}) collective-permute-start(bf16[16,2048]{1,0:T(8,128)(2,1)S(1)} %get-tuple-element.60), channel_id=1, source_target_pairs={{0,4},{4,0},{8,12},{12,8},{16,20},{20,16},{24,28},{28,24},{1,5},{5... | collective-permute-start | bytes 196616 | tf_op jit(solution)/shard_map/ppermute | solution.py:31
  88.3 4.3 %collective-permute-start.18 = (bf16[16,2048]{1,0:T(8,128)(2,1)S(1)}, bf16[16,2048]{1,0:T(8,128)(2,1)S(1)}, u32[]{:S(2)}, u32[]{:S(2)}) collective-permute-start(bf16[16,2048]{1,0:T(8,128)(2,1)S(1)} %get-tuple-element.61), channel_id=1, source_target_pairs={{0,8},{4,12},{8,0},{12,4},{16,24},{20,28},{24,16},{28,20},{1,9},{5... | collective-permute-start | bytes 196616 | tf_op jit(solution)/shard_map/ppermute | solution.py:31
  88.6 5.2 %collective-permute-start.19 = (bf16[16,2048]{1,0:T(8,128)(2,1)S(1)}, bf16[16,2048]{1,0:T(8,128)(2,1)S(1)}, u32[]{:S(2)}, u32[]{:S(2)}) collective-permute-start(bf16[16,2048]{1,0:T(8,128)(2,1)S(1)} %get-tuple-element.62), channel_id=1, source_target_pairs={{0,12},{4,8},{8,4},{12,0},{16,28},{20,24},{24,20},{28,16},{1,13},{... | collective-permute-start | bytes 196616 | tf_op jit(solution)/shard_map/ppermute | solution.py:31
  (8 other events, 85.9 us)
where the time goes:
time: 95 us; the launch traced here: 94.7 us
  starting transfers between devices  43.9 us (46%)
  waiting for transfers between devices  36.1 us (38%)
  Pallas kernels  14.6 us (15%)
    ppermute x37, starting transfers between devices, swap(): return lax.ppermute(x, axis, [(i, i ^ k) for i in range(n)])  43.9 us
    ppermute x37, waiting for transfers between devices, swap(): return lax.ppermute(x, axis, [(i, i ^ k) for i in range(n)])  36.1 us
    pallas_call x17, Pallas kernels, call(): pl.pallas_call(kernel, out_shape=shapes, in_specs=ins, out_specs=outs, sc...  14.6 us
  transfers between devices with their start and end apart: 37, of which 19 were waited for; matrix products, arithmetic and copies ran while one was open for 0% of the time, Pallas kernels for 10%

commit v1 on v0

--- a/solution.py
+++ b/solution.py
@@ -158,8 +158,7 @@
         ref[...] = jnp.dot(lhs, w_ref[...], preferred_element_type=F32).astype(ref.dtype)
 
 
-def pair_kernel(keep_ref, got_ref, *outs):
-    first = keep_ref.shape[0] // 2
+def pair_kernel(first, keep_ref, got_ref, *outs):
     for ref in outs:
         here = pl.ds(first, ref.shape[0])
         ref[...] = (keep_ref[here, :].astype(F32) + got_ref[here, :].astype(F32)).astype(ref.dtype)
@@ -201,7 +200,7 @@
         c.wait()
 
 
-def dispatch_kernel(cap, slot_ref, gain_ref, base_ref, r2_ref, hid_ref, *outs):
+def dispatch_kernel(cap, slot_ref, gain_ref, base_ref, r2_ref, hid_ref, near_ref, *outs):
     rows = base_ref.shape[0]
     hidden = base_ref[...] + r2_ref[...].astype(F32)
     hid_ref[...] = hidden
@@ -215,13 +214,46 @@
             hit = hit | (slot == slot_ref[j : j + 1, :])
         return jnp.dot(hit.astype(BF16), normed, preferred_element_type=F32).astype(BF16)
 
+    near = near_ref.shape[0]
     if cap % 16 == 0:
-        picked = pick(0, cap * len(outs))
+        picked = pick(0, near + cap * len(outs))
+        near_ref[...] = picked[:near]
         for k, ref in enumerate(outs):
-            ref[...] = picked[k * cap : (k + 1) * cap, :]
+            ref[...] = picked[near + k * cap : near + (k + 1) * cap, :]
     else:
+        near_ref[...] = pick(0, near)
         for k, ref in enumerate(outs):
-            ref[...] = pick(k * cap, cap)
+            ref[...] = pick(near + k * cap, cap)
+
+
+def fold_kernel(near_ref, got_ref, *outs):
+    cap = outs[0].shape[0] // 2
+    near, got = near_ref[...], got_ref[...]
+    for k, ref in enumerate(outs):
+        here = slice(k * cap, (k + 1) * cap)
+        ref[...] = jnp.concatenate([near[here], got[here]], axis=0)
+
+
+def near_pair_kernel(cap, keep_ref, got_ref, *outs):
+    first = 0
+    for ref in outs:
+        for k in range(ref.shape[0] // cap):
+            here = pl.ds(first + cap, cap)
+            ref[pl.ds(k * cap, cap), :] = (
+                keep_ref[here, :].astype(F32) + got_ref[here, :].astype(F32)
+            ).astype(BF16)
+            first += 2 * cap
+
+
+def near_settle_kernel(first, keep_ref, r1_ref, r2_ref, *outs):
+    for k, ref in enumerate(outs):
+        cap = ref.shape[0]
+        here = pl.ds(2 * cap * (first + k), cap)
+        ref[...] = (
+            keep_ref[here, :].astype(F32)
+            + r1_ref[here, :].astype(F32)
+            + r2_ref[pl.ds(k * cap, cap), :].astype(F32)
+        ).astype(BF16)
 
 
 def join_kernel(*refs):
@@ -308,7 +340,9 @@
     )
 
     half = sp_size // 2
-    pieces = [kv] + [swap(kv, "sp", k) for k in range(1, sp_size)]
+    far = swap(kv, "sp", half)
+    pieces = [kv] + [swap(kv, "sp", k) for k in range(1, half)]
+    pieces += [far] + [swap(far, "sp", k) for k in range(1, half)]
     if len(pieces) > 8:
         each = len(pieces) // 8
         pieces = [jnp.concatenate(pieces[i * each : (i + 1) * each], axis=0) for i in range(8)]
@@ -337,14 +371,18 @@
         16,
     )
 
-    def add_pair(kept, got, splits):
-        n = kept.shape[0] // (2 * splits)
+    def add_pair(kept, got, first, splits):
+        n = (kept.shape[0] - first) // splits
         return call(
-            pair_kernel, (kept, got), [VM] * 2, [VM] * splits, [shaped((n, width), BF16)] * splits
+            functools.partial(pair_kernel, first),
+            (kept, got),
+            [VM] * 2,
+            [VM] * splits,
+            [shaped((n, width), BF16)] * splits,
         )
 
     r1 = swap(send, "tp", 1)
-    (pair,) = add_pair(keep, r1, 1)
+    (pair,) = add_pair(keep, r1, own, 1)
     r2 = swap(pair, "tp", 2)
     slot, base, gain, mix, down = call(
         lambda *a: base_kernel(experts, cap, *a),
@@ -368,39 +406,23 @@
         ],
     )
 
+    near_rows = cap * half
     picked = call(
         lambda *a: dispatch_kernel(cap, *a),
         (slot, gain, base, r2),
         [VM] * 4,
-        [VM] * (1 + sp_size),
-        [shaped((own, width), F32)] + [shaped((cap, width), BF16)] * sp_size,
-    )
-    hidden, mail = picked[0], picked[1:]
-
-    inbox = [mail[0]] + [swap(mail[k], "sp", k) for k in range(1, sp_size)]
+        [VM] * (2 + half),
+        [shaped((own, width), F32), shaped((near_rows, width), BF16)]
+        + [shaped((cap, width), BF16)] * half,
+    )
+    hidden, near_block, mail = picked[0], picked[1], picked[2:]
     fe = expert_gate.shape[2]
     fc = 256 if fe % 256 == 0 else fe
-    returned = []
-    for c in range(2):
-        splits = 2 if c == 1 and half % 2 == 0 else 1
-        each = half // splits
-        n = cap * each
-        mine = [
-            call(
-                join_kernel,
-                inbox[c * half + i * each : c * half + (i + 1) * each],
-                [VM] * each,
-                VM,
-                shaped((n, width), BF16),
-            )
-            for i in range(splits)
-        ]
-        core = [swap(m, "tp", 1) for m in mine]
-        cross = [swap(m, "tp", 2) for m in mine]
-        both = [swap(m, "tp", 1) for m in cross]
-        rows_in = mine + cross + core + both
-        out = shaped((2 * cap * half, width), BF16)
-        keep_e, send_e = call(
+
+    def run(rows_in):
+        rows_all = sum(r.shape[0] for r in rows_in)
+        out = shaped((rows_all // 2, width), BF16)
+        return call(
             lambda *a: expert_kernel(len(rows_in), fc, *a),
             (*rows_in, expert_gate, expert_up, down),
             [VM] * (len(rows_in) + 3),
@@ -409,24 +431,74 @@
             (),
             24,
         )
-        e1 = swap(send_e, "tp", 1)
-        pairs = add_pair(keep_e, e1, splits)
-        for i, part in enumerate(pairs):
-            e2 = swap(part, "tp", 2)
-            settled = call(
-                functools.partial(settle_kernel, i * n),
-                (keep_e, e1, e2),
-                [VM] * 3,
-                [VM] * each,
-                [shaped((cap, width), BF16)] * each,
-            )
-            for k in range(each):
-                peer = c * half + i * each + k
-                returned.append(swap(settled[k], "sp", peer) if peer else settled[k])
+
+    def join(parts):
+        rows_all = sum(p.shape[0] for p in parts)
+        return call(join_kernel, parts, [VM] * len(parts), VM, shaped((rows_all, width), BF16))
+
+    splits = 2 if half % 2 == 0 else 1
+    each = half // splits
+    inbox = [swap(mail[k], "sp", half + k) for k in range(half)]
+    mine = [join(inbox[i * each : (i + 1) * each]) for i in range(splits)]
+    core = [swap(m, "tp", 1) for m in mine]
+    cross = [swap(m, "tp", 2) for m in mine]
+    both = [swap(m, "tp", 1) for m in cross]
+    keep_a, send_a = run(mine + core)
+    keep_b, send_b = run(cross + both)
+    e1a = swap(send_a, "tp", 1)
+    e1b = swap(send_b, "tp", 1)
+    pairs = add_pair(keep_b, e1b, 0, splits)
+    far_back = []
+    for i, part in enumerate(pairs):
+        e2 = swap(part, "tp", 2)
+        settled = call(
+            functools.partial(settle_kernel, i * each * cap),
+            (keep_a, e1a, e2),
+            [VM] * 3,
+            [VM] * each,
+            [shaped((cap, width), BF16)] * each,
+        )
+        for k, rows_k in enumerate(settled):
+            peer = half + i * each + k
+            far_back.append(swap(rows_k, "sp", peer))
+
+    got = swap(near_block, "tp", 2)
+    folded = call(
+        fold_kernel,
+        (near_block, got),
+        [VM] * 2,
+        [VM] * half,
+        [shaped((2 * cap, width), BF16)] * half,
+    )
+    inbox = [folded[0]] + [swap(folded[k], "sp", k) for k in range(1, half)]
+    mine0 = join(inbox)
+    core0 = swap(mine0, "tp", 1)
+    keep_n, send_n = run([mine0, core0])
+    e1 = swap(send_n, "tp", 1)
+    pairs = call(
+        functools.partial(near_pair_kernel, cap),
+        (keep_n, e1),
+        [VM] * 2,
+        [VM] * splits,
+        [shaped((cap * each, width), BF16)] * splits,
+    )
+    near_back = []
+    for i, part in enumerate(pairs):
+        e2 = swap(part, "tp", 2)
+        settled = call(
+            functools.partial(near_settle_kernel, i * each),
+            (keep_n, e1, e2),
+            [VM] * 3,
+            [VM] * each,
+            [shaped((cap, width), BF16)] * each,
+        )
+        for k, rows_k in enumerate(settled):
+            peer = i * each + k
+            near_back.append(swap(rows_k, "sp", peer) if peer else rows_k)
 
     return call(
         combine_kernel,
-        (slot, mix, hidden, *returned),
+        (slot, mix, hidden, *near_back, *far_back),
         [VM] * (3 + sp_size),
         VM,
         shaped((own, width), BF16),

time: 95 us -> 93.5 us (0.984)
  waiting for transfers between devices: 36.1 us -> 31.8 us
  starting transfers between devices: 43.9 us -> 45.4 us
  Pallas kernels: 14.6 us -> 16 us
    ppermute x37 -> x38, waiting for transfers between devices: 36.1 us -> 31.8 us  [swap(): return lax.ppermute(x, axis, [(i, i ^ k) for i in range(n)])]
    ppermute x37 -> x38, starting transfers between devices: 43.9 us -> 45.4 us  [swap(): return lax.ppermute(x, axis, [(i, i ^ k) for i in range(n)])]
    pallas_call x17 -> x20, Pallas kernels: 14.6 us -> 16 us  [call(): pl.pallas_call(kernel, out_shape=shapes, in_specs=ins, out_specs=outs, sc...]
  transfers between devices with their start and end apart: 37 -> 38, of which waited for: 19 -> 19; matrix products, arithmetic and copies ran while one was open for 0% -> 0% of each run, Pallas kernels for 10% -> 12%
where the time goes in v1:
time: 93.5 us; the launch traced here: 93.3 us
  starting transfers between devices  45.4 us (49%)
  waiting for transfers between devices  31.8 us (34%)
  Pallas kernels  16 us (17%)
    ppermute x38, starting transfers between devices, swap(): return lax.ppermute(x, axis, [(i, i ^ k) for i in range(n)])  45.4 us
    ppermute x38, waiting for transfers between devices, swap(): return lax.ppermute(x, axis, [(i, i ^ k) for i in range(n)])  31.8 us
    pallas_call x20, Pallas kernels, call(): pl.pallas_call(kernel, out_shape=shapes, in_specs=ins, out_specs=outs, sc...  16 us
  transfers between devices with their start and end apart: 38, of which 19 were waited for; matrix products, arithmetic and copies ran while one was open for 0% of the time, Pallas kernels for 12%

profile of v1, /device:TPU:0, one launch (start us, length us, event | category | flops | bytes accessed | tf_op | source)
XLA Modules:
  0.0 93.3 jit_solution(3759905446862841921)
XLA Ops:
  1.0 4.1 %collective-permute-start.3 = (bf16[128,256]{1,0:T(8,128)(2,1)S(1)}, bf16[128,256]{1,0:T(8,128)(2,1)S(1)}, u32[]{:S(2)}, u32[]{:S(2)}) collective-permute-start(bf16[128,256]{1,0:T(8,128)(2,1)S(1)} %get-tuple-element.49.a_3_), channel_id=1, source_target_pairs={{0,16},{4,20},{8,24},{12,28},{16,0},{20,4},{24,8},{28,12},{1,17},{... | collective-permute-start | bytes 196616 | tf_op jit(solution)/shard_map/ppermute | solution.py:31
  5.1 2.5 %collective-permute-start.2 = (bf16[128,256]{1,0:T(8,128)(2,1)S(1)}, bf16[128,256]{1,0:T(8,128)(2,1)S(1)}, u32[]{:S(2)}, u32[]{:S(2)}) collective-permute-start(bf16[128,256]{1,0:T(8,128)(2,1)S(1)} %get-tuple-element.49.a_3_), channel_id=1, source_target_pairs={{0,12},{4,8},{8,4},{12,0},{16,28},{20,24},{24,20},{28,16},{1,13},{... | collective-permute-start | bytes 196616 | tf_op jit(solution)/shard_map/ppermute | solution.py:31
  8.6 2.5 %collective-permute-start.6 = (bf16[128,256]{1,0:T(8,128)(2,1)S(1)}, bf16[128,256]{1,0:T(8,128)(2,1)S(1)}, u32[]{:S(2)}, u32[]{:S(2)}) collective-permute-start(bf16[128,256]{1,0:T(8,128)(2,1)S(1)} %collective-permute-done.3.a_7_), channel_id=1, source_target_pairs={{0,12},{4,8},{8,4},{12,0},{16,28},{20,24},{24,20},{28,16},{1,13},{... | collective-permute-start | bytes 196616 | tf_op jit(solution)/shard_map/ppermute | solution.py:31
  12.5 1.7 %shard_map.128 = (bf16[512,128]{1,0:T(8,128)(2,1)S(1)}, bf16[512,2048]{1,0:T(8,128)(2,1)S(1)}) custom-call(f32[128,128]{1,0:T(8,128)S(1)} %get-tuple-element.45.cos_ref, f32[128,128]{1,0:T(8,128)S(1)} %get-tuple-element.46.sin_ref, f32[1,128]{1,0:T(1,128)} %bitcast.11, bf16[128,512]{1,0:T(8,128)(2,1)} %q_ref.1, bf16[512,2048]{1,0:T(8,128)(2,1)} %w_ref.1), custom_call_target="tpu_custom_call" | custom-call | tf_op jit(solution)/shard_map/pallas_call | solution.py:39
  15.9 2.4 %shard_map.129 = (f32[64,2048]{1,0:T(8,128)S(1)}, bf16[64,2048]{1,0:T(8,128)(2,1)S(1)}) custom-call(s32[1]{0:T(128)} %bitcast.1.a_0_, bf16[512,128]{1,0:T(8,128)(2,1)S(1)} %get-tuple-element.47.a_1_, bf16[512,2048]{1,0:T(8,128)(2,1)S(1)} %get-tuple-element.48.a_2_, bf16[128,256]{1,0:T(8,128)(2,1)S(1)} %get-tuple-element.49.a_3_, ...), custom_call_target="tpu_custom_call" | custom-call | tf_op jit(solution)/shard_map/pallas_call | solution.py:39
  18.3 1.5 %collective-permute-done.7.got_ref.a_8_ = bf16[64,2048]{1,0:T(8,128)(2,1)S(1)} collective-permute-done((bf16[64,2048]{1,0:T(8,128)(2,1)S(1)}, bf16[64,2048]{1,0:T(8,128)(2,1)S(1)}, u32[]{:S(2)}, u32[]{:S(2)}) %collective-permute-start.7) | collective-permute-done | bytes 262176 | tf_op jit(solution)/shard_map/ppermute | solution.py:31
  19.9 1.6 %collective-permute-start.8 = (bf16[32,2048]{1,0:T(8,128)(2,1)S(1)}, bf16[32,2048]{1,0:T(8,128)(2,1)S(1)}, u32[]{:S(2)}, u32[]{:S(2)}) collective-permute-start(bf16[32,2048]{1,0:T(8,128)(2,1)S(1)} %shard_map.130.a_1_), channel_id=1, source_target_pairs={{0,2},{1,3},{2,0},{3,1},{4,6},{5,7},{6,4},{7,5},{8,10},{9,11},{10,... | collective-permute-start | bytes 393224 | tf_op jit(solution)/shard_map/ppermute | solution.py:31
  21.5 2.2 %shard_map.131 = (s32[2,32]{1,0:T(2,128)S(1)}, f32[32,2048]{1,0:T(8,128)S(1)}, f32[1,2048]{1,0:T(1,128)S(1)}, f32[2,32]{1,0:T(2,128)S(1)}, bf16[1,768,2048]{2,1,0:T(8,128)(2,1)S(1)}) custom-call(s32[1]{0:T(128)} %bitcast.sp_ref.a_0_, bf16[32,2048]{1,0:T(8,128)(2,1)} %copy-done.2, s32[2,32]{1,0:T(2,128)} %bitcast.8, bf16[32,2048]{1,0:T(8,128)(2,1)} %a_3_.2, ...), custom_call_target="tpu_custom_call" | custom-call | tf_op jit(solution)/shard_map/pallas_call | solution.py:39
  23.7 1.8 %collective-permute-done.8.a_3_ = bf16[32,2048]{1,0:T(8,128)(2,1)S(1)} collective-permute-done((bf16[32,2048]{1,0:T(8,128)(2,1)S(1)}, bf16[32,2048]{1,0:T(8,128)(2,1)S(1)}, u32[]{:S(2)}, u32[]{:S(2)}) %collective-permute-start.8) | collective-permute-done | bytes 131104 | tf_op jit(solution)/shard_map/ppermute | solution.py:31
  25.9 1.6 %collective-permute-start.9 = (bf16[64,2048]{1,0:T(8,128)(2,1)S(1)}, bf16[64,2048]{1,0:T(8,128)(2,1)S(1)}, u32[]{:S(2)}, u32[]{:S(2)}) collective-permute-start(bf16[64,2048]{1,0:T(8,128)(2,1)S(1)} %get-tuple-element.57.near_ref), channel_id=1, source_target_pairs={{0,2},{1,3},{2,0},{3,1},{4,6},{5,7},{6,4},{7,5},{8,10},{9,11},{10,... | collective-permute-start | bytes 786440 | tf_op jit(solution)/shard_map/ppermute | solution.py:31
  27.5 6.0 %collective-permute-done.9.got_ref = bf16[64,2048]{1,0:T(8,128)(2,1)S(1)} collective-permute-done((bf16[64,2048]{1,0:T(8,128)(2,1)S(1)}, bf16[64,2048]{1,0:T(8,128)(2,1)S(1)}, u32[]{:S(2)}, u32[]{:S(2)}) %collective-permute-start.9) | collective-permute-done | bytes 262176 | tf_op jit(solution)/shard_map/ppermute | solution.py:31
  37.1 2.9 %collective-permute-done.10.refs_1_ = bf16[32,2048]{1,0:T(8,128)(2,1)S(1)} collective-permute-done((bf16[32,2048]{1,0:T(8,128)(2,1)S(1)}, bf16[32,2048]{1,0:T(8,128)(2,1)S(1)}, u32[]{:S(2)}, u32[]{:S(2)}) %collective-permute-start.10) | collective-permute-done | bytes 131104 | tf_op jit(solution)/shard_map/ppermute | solution.py:31
  39.9 1.6 %collective-permute-done.12.refs_3_ = bf16[32,2048]{1,0:T(8,128)(2,1)S(1)} collective-permute-done((bf16[32,2048]{1,0:T(8,128)(2,1)S(1)}, bf16[32,2048]{1,0:T(8,128)(2,1)S(1)}, u32[]{:S(2)}, u32[]{:S(2)}) %collective-permute-start.12) | collective-permute-done | bytes 131104 | tf_op jit(solution)/shard_map/ppermute | solution.py:31
  41.6 3.5 %collective-permute-start.22 = (bf16[16,2048]{1,0:T(8,128)(2,1)S(1)}, bf16[16,2048]{1,0:T(8,128)(2,1)S(1)}, u32[]{:S(2)}, u32[]{:S(2)}) collective-permute-start(bf16[16,2048]{1,0:T(8,128)(2,1)S(1)} %get-tuple-element.73), channel_id=1, source_target_pairs={{0,24},{4,28},{8,16},{12,20},{16,8},{20,12},{24,0},{28,4},{1,25},{... | collective-permute-start | bytes 196616 | tf_op jit(solution)/shard_map/ppermute | solution.py:31
  47.2 2.1 %collective-permute-start.21 = (bf16[16,2048]{1,0:T(8,128)(2,1)S(1)}, bf16[16,2048]{1,0:T(8,128)(2,1)S(1)}, u32[]{:S(2)}, u32[]{:S(2)}) collective-permute-start(bf16[16,2048]{1,0:T(8,128)(2,1)S(1)} %get-tuple-element.72), channel_id=1, source_target_pairs={{0,20},{4,16},{8,28},{12,24},{16,4},{20,0},{24,12},{28,8},{1,21},{... | collective-permute-start | bytes 196616 | tf_op jit(solution)/shard_map/ppermute | solution.py:31
  49.4 3.4 %collective-permute-done.23.refs_1_ = bf16[16,2048]{1,0:T(8,128)(2,1)S(1)} collective-permute-done((bf16[16,2048]{1,0:T(8,128)(2,1)S(1)}, bf16[16,2048]{1,0:T(8,128)(2,1)S(1)}, u32[]{:S(2)}, u32[]{:S(2)}) %collective-permute-start.23) | collective-permute-done | bytes 65568 | tf_op jit(solution)/shard_map/ppermute | solution.py:31
  52.8 1.6 %collective-permute-start.28 = (bf16[32,2048]{1,0:T(8,128)(2,1)S(1)}, bf16[32,2048]{1,0:T(8,128)(2,1)S(1)}, u32[]{:S(2)}, u32[]{:S(2)}) collective-permute-start(bf16[32,2048]{1,0:T(8,128)(2,1)S(1)} %shard_map.140.a_1_), channel_id=1, source_target_pairs={{0,2},{1,3},{2,0},{3,1},{4,6},{5,7},{6,4},{7,5},{8,10},{9,11},{10,... | collective-permute-start | bytes 393224 | tf_op jit(solution)/shard_map/ppermute | solution.py:31
  55.5 2.2 %collective-permute-done.21.refs_1_ = bf16[16,2048]{1,0:T(8,128)(2,1)S(1)} collective-permute-done((bf16[16,2048]{1,0:T(8,128)(2,1)S(1)}, bf16[16,2048]{1,0:T(8,128)(2,1)S(1)}, u32[]{:S(2)}, u32[]{:S(2)}) %collective-permute-start.21) | collective-permute-done | bytes 65568 | tf_op jit(solution)/shard_map/ppermute | solution.py:31
  57.7 1.6 %collective-permute-start.27 = (bf16[32,2048]{1,0:T(8,128)(2,1)S(1)}, bf16[32,2048]{1,0:T(8,128)(2,1)S(1)}, u32[]{:S(2)}, u32[]{:S(2)}) collective-permute-start(bf16[32,2048]{1,0:T(8,128)(2,1)S(1)} %shard_map.139.a_0_), channel_id=1, source_target_pairs={{0,2},{1,3},{2,0},{3,1},{4,6},{5,7},{6,4},{7,5},{8,10},{9,11},{10,... | collective-permute-start | bytes 393224 | tf_op jit(solution)/shard_map/ppermute | solution.py:31
  59.3 2.7 %shard_map.135 = (bf16[128,2048]{1,0:T(8,128)(2,1)S(1)}, bf16[128,2048]{1,0:T(8,128)(2,1)S(1)}) custom-call(bf16[128,2048]{1,0:T(8,128)(2,1)S(1)} %shard_map.134.a_0_, bf16[128,2048]{1,0:T(8,128)(2,1)S(1)} %collective-permute-done.13.a_1_, bf16[1,2048,768]{2,1,0:T(8,128)(2,1)S(1)} %copy-done, bf16[1,2048,768]{2,1,0:T(8,128)(2,1)S(1)} %copy-done.1, ...), custom_call_target="tpu_custom_call" | custom-call | tf_op jit(solution)/shard_map/pallas_call | solution.py:39
  64.4 2.1 %shard_map.142 = (bf16[64,2048]{1,0:T(8,128)(2,1)S(1)}, bf16[64,2048]{1,0:T(8,128)(2,1)S(1)}) custom-call(bf16[32,2048]{1,0:T(8,128)(2,1)S(1)} %collective-permute-done.27.a_0_, bf16[32,2048]{1,0:T(8,128)(2,1)S(1)} %collective-permute-done.28.a_1_, bf16[32,2048]{1,0:T(8,128)(2,1)S(1)} %collective-permute-done.29.a_2_, ...), custom_call_target="tpu_custom_call" | custom-call | tf_op jit(solution)/shard_map/pallas_call | solution.py:39
  66.7 2.1 %shard_map.141 = (bf16[64,2048]{1,0:T(8,128)(2,1)S(1)}, bf16[64,2048]{1,0:T(8,128)(2,1)S(1)}) custom-call(bf16[32,2048]{1,0:T(8,128)(2,1)S(1)} %shard_map.139.a_0_, bf16[32,2048]{1,0:T(8,128)(2,1)S(1)} %shard_map.140.a_1_, bf16[32,2048]{1,0:T(8,128)(2,1)S(1)} %collective-permute-done.24.a_2_, bf16[32,2048]{1,0:T(8,128)(2,1)S(1)} %collective-permute-done.25.a_3_, ...), custom_call_target="tpu_custom_call" | custom-call | tf_op jit(solution)/shard_map/pallas_call | solution.py:39
  69.3 1.6 %collective-permute-start.32 = (bf16[32,2048]{1,0:T(8,128)(2,1)S(1)}, bf16[32,2048]{1,0:T(8,128)(2,1)S(1)}, u32[]{:S(2)}, u32[]{:S(2)}) collective-permute-start(bf16[32,2048]{1,0:T(8,128)(2,1)S(1)} %get-tuple-element.79), channel_id=1, source_target_pairs={{0,2},{1,3},{2,0},{3,1},{4,6},{5,7},{6,4},{7,5},{8,10},{9,11},{10,... | collective-permute-start | bytes 393224 | tf_op jit(solution)/shard_map/ppermute | solution.py:31
  71.5 1.6 %collective-permute-start.15 = (bf16[32,2048]{1,0:T(8,128)(2,1)S(1)}, bf16[32,2048]{1,0:T(8,128)(2,1)S(1)}, u32[]{:S(2)}, u32[]{:S(2)}) collective-permute-start(bf16[32,2048]{1,0:T(8,128)(2,1)S(1)} %get-tuple-element.65), channel_id=1, source_target_pairs={{0,2},{1,3},{2,0},{3,1},{4,6},{5,7},{6,4},{7,5},{8,10},{9,11},{10,... | collective-permute-start | bytes 393224 | tf_op jit(solution)/shard_map/ppermute | solution.py:31
  73.6 2.2 %collective-permute-done.32.r2_ref = bf16[32,2048]{1,0:T(8,128)(2,1)S(1)} collective-permute-done((bf16[32,2048]{1,0:T(8,128)(2,1)S(1)}, bf16[32,2048]{1,0:T(8,128)(2,1)S(1)}, u32[]{:S(2)}, u32[]{:S(2)}) %collective-permute-start.32) | collective-permute-done | bytes 131104 | tf_op jit(solution)/shard_map/ppermute | solution.py:31
  75.8 1.5 %collective-permute-start.33 = (bf16[16,2048]{1,0:T(8,128)(2,1)S(1)}, bf16[16,2048]{1,0:T(8,128)(2,1)S(1)}, u32[]{:S(2)}, u32[]{:S(2)}) collective-permute-start(bf16[16,2048]{1,0:T(8,128)(2,1)S(1)} %get-tuple-element.80), channel_id=1, source_target_pairs={{0,16},{4,20},{8,24},{12,28},{16,0},{20,4},{24,8},{28,12},{1,17},{... | collective-permute-start | bytes 196616 | tf_op jit(solution)/shard_map/ppermute | solution.py:31
  77.3 1.8 %collective-permute-start.34 = (bf16[16,2048]{1,0:T(8,128)(2,1)S(1)}, bf16[16,2048]{1,0:T(8,128)(2,1)S(1)}, u32[]{:S(2)}, u32[]{:S(2)}) collective-permute-start(bf16[16,2048]{1,0:T(8,128)(2,1)S(1)} %get-tuple-element.81), channel_id=1, source_target_pairs={{0,20},{4,16},{8,28},{12,24},{16,4},{20,0},{24,12},{28,8},{1,21},{... | collective-permute-start | bytes 196616 | tf_op jit(solution)/shard_map/ppermute | solution.py:31
  79.1 2.4 %collective-permute-start.36 = (bf16[16,2048]{1,0:T(8,128)(2,1)S(1)}, bf16[16,2048]{1,0:T(8,128)(2,1)S(1)}, u32[]{:S(2)}, u32[]{:S(2)}) collective-permute-start(bf16[16,2048]{1,0:T(8,128)(2,1)S(1)} %get-tuple-element.83), channel_id=1, source_target_pairs={{0,24},{4,28},{8,16},{12,20},{16,8},{20,12},{24,0},{28,4},{1,25},{... | collective-permute-start | bytes 196616 | tf_op jit(solution)/shard_map/ppermute | solution.py:31
  81.5 2.4 %collective-permute-start.37 = (bf16[16,2048]{1,0:T(8,128)(2,1)S(1)}, bf16[16,2048]{1,0:T(8,128)(2,1)S(1)}, u32[]{:S(2)}, u32[]{:S(2)}) collective-permute-start(bf16[16,2048]{1,0:T(8,128)(2,1)S(1)} %get-tuple-element.84), channel_id=1, source_target_pairs={{0,28},{4,24},{8,20},{12,16},{16,12},{20,8},{24,4},{28,0},{1,29},{... | collective-permute-start | bytes 196616 | tf_op jit(solution)/shard_map/ppermute | solution.py:31
  84.1 1.5 %collective-permute-start.16 = (bf16[16,2048]{1,0:T(8,128)(2,1)S(1)}, bf16[16,2048]{1,0:T(8,128)(2,1)S(1)}, u32[]{:S(2)}, u32[]{:S(2)}) collective-permute-start(bf16[16,2048]{1,0:T(8,128)(2,1)S(1)} %get-tuple-element.67), channel_id=1, source_target_pairs={{0,4},{4,0},{8,12},{12,8},{16,20},{20,16},{24,28},{28,24},{1,5},{5... | collective-permute-start | bytes 196616 | tf_op jit(solution)/shard_map/ppermute | solution.py:31
  85.7 1.5 %collective-permute-done.34.refs_5_ = bf16[16,2048]{1,0:T(8,128)(2,1)S(1)} collective-permute-done((bf16[16,2048]{1,0:T(8,128)(2,1)S(1)}, bf16[16,2048]{1,0:T(8,128)(2,1)S(1)}, u32[]{:S(2)}, u32[]{:S(2)}) %collective-permute-start.34) | collective-permute-done | bytes 65568 | tf_op jit(solution)/shard_map/ppermute | solution.py:31
  89.9 2.4 %collective-permute-done.19.refs_3_ = bf16[16,2048]{1,0:T(8,128)(2,1)S(1)} collective-permute-done((bf16[16,2048]{1,0:T(8,128)(2,1)S(1)}, bf16[16,2048]{1,0:T(8,128)(2,1)S(1)}, u32[]{:S(2)}, u32[]{:S(2)}) %collective-permute-start.19) | collective-permute-done | bytes 65568 | tf_op jit(solution)/shard_map/ppermute | solution.py:31
  (70 shorter events, 20.6 us)
Async XLA Ops:
  1.0 7.6 %collective-permute-start.3 = (bf16[128,256]{1,0:T(8,128)(2,1)S(1)}, bf16[128,256]{1,0:T(8,128)(2,1)S(1)}, u32[]{:S(2)}, u32[]{:S(2)}) collective-permute-start(bf16[128,256]{1,0:T(8,128)(2,1)S(1)} %get-tuple-element.49.a_3_), channel_id=1, source_target_pairs={{0,16},{4,20},{8,24},{12,28},{16,0},{20,4},{24,8},{28,12},{1,17},{... | collective-permute-start | bytes 196616 | tf_op jit(solution)/shard_map/ppermute | solution.py:31
  5.1 6.5 %collective-permute-start.2 = (bf16[128,256]{1,0:T(8,128)(2,1)S(1)}, bf16[128,256]{1,0:T(8,128)(2,1)S(1)}, u32[]{:S(2)}, u32[]{:S(2)}) collective-permute-start(bf16[128,256]{1,0:T(8,128)(2,1)S(1)} %get-tuple-element.49.a_3_), channel_id=1, source_target_pairs={{0,12},{4,8},{8,4},{12,0},{16,28},{20,24},{24,20},{28,16},{1,13},{... | collective-permute-start | bytes 196616 | tf_op jit(solution)/shard_map/ppermute | solution.py:31
  7.7 6.6 %collective-permute-start.1 = (bf16[128,256]{1,0:T(8,128)(2,1)S(1)}, bf16[128,256]{1,0:T(8,128)(2,1)S(1)}, u32[]{:S(2)}, u32[]{:S(2)}) collective-permute-start(bf16[128,256]{1,0:T(8,128)(2,1)S(1)} %get-tuple-element.49.a_3_), channel_id=1, source_target_pairs={{0,8},{4,12},{8,0},{12,4},{16,24},{20,28},{24,16},{28,20},{1,9},{5... | collective-permute-start | bytes 196616 | tf_op jit(solution)/shard_map/ppermute | solution.py:31
  8.1 6.2 %collective-permute-start = (bf16[128,256]{1,0:T(8,128)(2,1)S(1)}, bf16[128,256]{1,0:T(8,128)(2,1)S(1)}, u32[]{:S(2)}, u32[]{:S(2)}) collective-permute-start(bf16[128,256]{1,0:T(8,128)(2,1)S(1)} %get-tuple-element.49.a_3_), channel_id=1, source_target_pairs={{0,4},{4,0},{8,12},{12,8},{16,20},{20,16},{24,28},{28,24},{1,5},{5... | collective-permute-start | bytes 196616 | tf_op jit(solution)/shard_map/ppermute | solution.py:31
  8.6 5.7 %collective-permute-start.6 = (bf16[128,256]{1,0:T(8,128)(2,1)S(1)}, bf16[128,256]{1,0:T(8,128)(2,1)S(1)}, u32[]{:S(2)}, u32[]{:S(2)}) collective-permute-start(bf16[128,256]{1,0:T(8,128)(2,1)S(1)} %collective-permute-done.3.a_7_), channel_id=1, source_target_pairs={{0,12},{4,8},{8,4},{12,0},{16,28},{20,24},{24,20},{28,16},{1,13},{... | collective-permute-start | bytes 196616 | tf_op jit(solution)/shard_map/ppermute | solution.py:31
  11.1 4.3 %collective-permute-start.5 = (bf16[128,256]{1,0:T(8,128)(2,1)S(1)}, bf16[128,256]{1,0:T(8,128)(2,1)S(1)}, u32[]{:S(2)}, u32[]{:S(2)}) collective-permute-start(bf16[128,256]{1,0:T(8,128)(2,1)S(1)} %collective-permute-done.3.a_7_), channel_id=1, source_target_pairs={{0,8},{4,12},{8,0},{12,4},{16,24},{20,28},{24,16},{28,20},{1,9},{5... | collective-permute-start | bytes 196616 | tf_op jit(solution)/shard_map/ppermute | solution.py:31
  11.6 4.3 %collective-permute-start.4 = (bf16[128,256]{1,0:T(8,128)(2,1)S(1)}, bf16[128,256]{1,0:T(8,128)(2,1)S(1)}, u32[]{:S(2)}, u32[]{:S(2)}) collective-permute-start(bf16[128,256]{1,0:T(8,128)(2,1)S(1)} %collective-permute-done.3.a_7_), channel_id=1, source_target_pairs={{0,4},{4,0},{8,12},{12,8},{16,20},{20,16},{24,28},{28,24},{1,5},{5... | collective-permute-start | bytes 196616 | tf_op jit(solution)/shard_map/ppermute | solution.py:31
  19.9 5.6 %collective-permute-start.8 = (bf16[32,2048]{1,0:T(8,128)(2,1)S(1)}, bf16[32,2048]{1,0:T(8,128)(2,1)S(1)}, u32[]{:S(2)}, u32[]{:S(2)}) collective-permute-start(bf16[32,2048]{1,0:T(8,128)(2,1)S(1)} %shard_map.130.a_1_), channel_id=1, source_target_pairs={{0,2},{1,3},{2,0},{3,1},{4,6},{5,7},{6,4},{7,5},{8,10},{9,11},{10,... | collective-permute-start | bytes 393224 | tf_op jit(solution)/shard_map/ppermute | solution.py:31
  25.9 7.6 %collective-permute-start.9 = (bf16[64,2048]{1,0:T(8,128)(2,1)S(1)}, bf16[64,2048]{1,0:T(8,128)(2,1)S(1)}, u32[]{:S(2)}, u32[]{:S(2)}) collective-permute-start(bf16[64,2048]{1,0:T(8,128)(2,1)S(1)} %get-tuple-element.57.near_ref), channel_id=1, source_target_pairs={{0,2},{1,3},{2,0},{3,1},{4,6},{5,7},{6,4},{7,5},{8,10},{9,11},{10,... | collective-permute-start | bytes 786440 | tf_op jit(solution)/shard_map/ppermute | solution.py:31
  33.5 6.4 %collective-permute-start.10 = (bf16[32,2048]{1,0:T(8,128)(2,1)S(1)}, bf16[32,2048]{1,0:T(8,128)(2,1)S(1)}, u32[]{:S(2)}, u32[]{:S(2)}) collective-permute-start(bf16[32,2048]{1,0:T(8,128)(2,1)S(1)} %get-tuple-element.59), channel_id=1, source_target_pairs={{0,4},{4,0},{8,12},{12,8},{16,20},{20,16},{24,28},{28,24},{1,5},{5... | collective-permute-start | bytes 393224 | tf_op jit(solution)/shard_map/ppermute | solution.py:31
  34.5 5.4 %collective-permute-start.11 = (bf16[32,2048]{1,0:T(8,128)(2,1)S(1)}, bf16[32,2048]{1,0:T(8,128)(2,1)S(1)}, u32[]{:S(2)}, u32[]{:S(2)}) collective-permute-start(bf16[32,2048]{1,0:T(8,128)(2,1)S(1)} %get-tuple-element.60), channel_id=1, source_target_pairs={{0,8},{4,12},{8,0},{12,4},{16,24},{20,28},{24,16},{28,20},{1,9},{5... | collective-permute-start | bytes 393224 | tf_op jit(solution)/shard_map/ppermute | solution.py:31
  35.7 5.9 %collective-permute-start.12 = (bf16[32,2048]{1,0:T(8,128)(2,1)S(1)}, bf16[32,2048]{1,0:T(8,128)(2,1)S(1)}, u32[]{:S(2)}, u32[]{:S(2)}) collective-permute-start(bf16[32,2048]{1,0:T(8,128)(2,1)S(1)} %get-tuple-element.61), channel_id=1, source_target_pairs={{0,12},{4,8},{8,4},{12,0},{16,28},{20,24},{24,20},{28,16},{1,13},{... | collective-permute-start | bytes 393224 | tf_op jit(solution)/shard_map/ppermute | solution.py:31
  41.6 17.7 %collective-permute-start.13 = (bf16[128,2048]{1,0:T(8,128)(2,1)S(1)}, bf16[128,2048]{1,0:T(8,128)(2,1)S(1)}, u32[]{:S(2)}, u32[]{:S(2)}) collective-permute-start(bf16[128,2048]{1,0:T(8,128)(2,1)S(1)} %shard_map.134.a_0_), channel_id=1, source_target_pairs={{0,1},{1,0},{2,3},{3,2},{4,5},{5,4},{6,7},{7,6},{8,9},{9,8},{10,11... | collective-permute-start | bytes 1572872 | tf_op jit(solution)/shard_map/ppermute | solution.py:31
  41.6 7.7 %collective-permute-start.22 = (bf16[16,2048]{1,0:T(8,128)(2,1)S(1)}, bf16[16,2048]{1,0:T(8,128)(2,1)S(1)}, u32[]{:S(2)}, u32[]{:S(2)}) collective-permute-start(bf16[16,2048]{1,0:T(8,128)(2,1)S(1)} %get-tuple-element.73), channel_id=1, source_target_pairs={{0,24},{4,28},{8,16},{12,20},{16,8},{20,12},{24,0},{28,4},{1,25},{... | collective-permute-start | bytes 196616 | tf_op jit(solution)/shard_map/ppermute | solution.py:31
  45.2 7.6 %collective-permute-start.23 = (bf16[16,2048]{1,0:T(8,128)(2,1)S(1)}, bf16[16,2048]{1,0:T(8,128)(2,1)S(1)}, u32[]{:S(2)}, u32[]{:S(2)}) collective-permute-start(bf16[16,2048]{1,0:T(8,128)(2,1)S(1)} %get-tuple-element.74), channel_id=1, source_target_pairs={{0,28},{4,24},{8,20},{12,16},{16,12},{20,8},{24,4},{28,0},{1,29},{... | collective-permute-start | bytes 196616 | tf_op jit(solution)/shard_map/ppermute | solution.py:31
  46.5 9.0 %collective-permute-start.20 = (bf16[16,2048]{1,0:T(8,128)(2,1)S(1)}, bf16[16,2048]{1,0:T(8,128)(2,1)S(1)}, u32[]{:S(2)}, u32[]{:S(2)}) collective-permute-start(bf16[16,2048]{1,0:T(8,128)(2,1)S(1)} %get-tuple-element.71), channel_id=1, source_target_pairs={{0,16},{4,20},{8,24},{12,28},{16,0},{20,4},{24,8},{28,12},{1,17},{... | collective-permute-start | bytes 196616 | tf_op jit(solution)/shard_map/ppermute | solution.py:31
  47.2 10.5 %collective-permute-start.21 = (bf16[16,2048]{1,0:T(8,128)(2,1)S(1)}, bf16[16,2048]{1,0:T(8,128)(2,1)S(1)}, u32[]{:S(2)}, u32[]{:S(2)}) collective-permute-start(bf16[16,2048]{1,0:T(8,128)(2,1)S(1)} %get-tuple-element.72), channel_id=1, source_target_pairs={{0,20},{4,16},{8,28},{12,24},{16,4},{20,0},{24,12},{28,8},{1,21},{... | collective-permute-start | bytes 196616 | tf_op jit(solution)/shard_map/ppermute | solution.py:31
  52.8 9.3 %collective-permute-start.28 = (bf16[32,2048]{1,0:T(8,128)(2,1)S(1)}, bf16[32,2048]{1,0:T(8,128)(2,1)S(1)}, u32[]{:S(2)}, u32[]{:S(2)}) collective-permute-start(bf16[32,2048]{1,0:T(8,128)(2,1)S(1)} %shard_map.140.a_1_), channel_id=1, source_target_pairs={{0,2},{1,3},{2,0},{3,1},{4,6},{5,7},{6,4},{7,5},{8,10},{9,11},{10,... | collective-permute-start | bytes 393224 | tf_op jit(solution)/shard_map/ppermute | solution.py:31
  57.7 5.3 %collective-permute-start.27 = (bf16[32,2048]{1,0:T(8,128)(2,1)S(1)}, bf16[32,2048]{1,0:T(8,128)(2,1)S(1)}, u32[]{:S(2)}, u32[]{:S(2)}) collective-permute-start(bf16[32,2048]{1,0:T(8,128)(2,1)S(1)} %shard_map.139.a_0_), channel_id=1, source_target_pairs={{0,2},{1,3},{2,0},{3,1},{4,6},{5,7},{6,4},{7,5},{8,10},{9,11},{10,... | collective-permute-start | bytes 393224 | tf_op jit(solution)/shard_map/ppermute | solution.py:31
  62.0 9.4 %collective-permute-start.14 = (bf16[128,2048]{1,0:T(8,128)(2,1)S(1)}, bf16[128,2048]{1,0:T(8,128)(2,1)S(1)}, u32[]{:S(2)}, u32[]{:S(2)}) collective-permute-start(bf16[128,2048]{1,0:T(8,128)(2,1)S(1)} %get-tuple-element.64), channel_id=1, source_target_pairs={{0,1},{1,0},{2,3},{3,2},{4,5},{5,4},{6,7},{7,6},{8,9},{9,8},{10,11... | collective-permute-start | bytes 1572872 | tf_op jit(solution)/shard_map/ppermute | solution.py:31
  68.8 4.8 %collective-permute-start.26 = (bf16[64,2048]{1,0:T(8,128)(2,1)S(1)}, bf16[64,2048]{1,0:T(8,128)(2,1)S(1)}, u32[]{:S(2)}, u32[]{:S(2)}) collective-permute-start(bf16[64,2048]{1,0:T(8,128)(2,1)S(1)} %get-tuple-element.76), channel_id=1, source_target_pairs={{0,1},{1,0},{2,3},{3,2},{4,5},{5,4},{6,7},{7,6},{8,9},{9,8},{10,11... | collective-permute-start | bytes 786440 | tf_op jit(solution)/shard_map/ppermute | solution.py:31
  69.3 6.4 %collective-permute-start.32 = (bf16[32,2048]{1,0:T(8,128)(2,1)S(1)}, bf16[32,2048]{1,0:T(8,128)(2,1)S(1)}, u32[]{:S(2)}, u32[]{:S(2)}) collective-permute-start(bf16[32,2048]{1,0:T(8,128)(2,1)S(1)} %get-tuple-element.79), channel_id=1, source_target_pairs={{0,2},{1,3},{2,0},{3,1},{4,6},{5,7},{6,4},{7,5},{8,10},{9,11},{10,... | collective-permute-start | bytes 393224 | tf_op jit(solution)/shard_map/ppermute | solution.py:31
  70.9 8.2 %collective-permute-start.35 = (bf16[32,2048]{1,0:T(8,128)(2,1)S(1)}, bf16[32,2048]{1,0:T(8,128)(2,1)S(1)}, u32[]{:S(2)}, u32[]{:S(2)}) collective-permute-start(bf16[32,2048]{1,0:T(8,128)(2,1)S(1)} %get-tuple-element.82), channel_id=1, source_target_pairs={{0,2},{1,3},{2,0},{3,1},{4,6},{5,7},{6,4},{7,5},{8,10},{9,11},{10,... | collective-permute-start | bytes 393224 | tf_op jit(solution)/shard_map/ppermute | solution.py:31
  71.5 10.1 %collective-permute-start.15 = (bf16[32,2048]{1,0:T(8,128)(2,1)S(1)}, bf16[32,2048]{1,0:T(8,128)(2,1)S(1)}, u32[]{:S(2)}, u32[]{:S(2)}) collective-permute-start(bf16[32,2048]{1,0:T(8,128)(2,1)S(1)} %get-tuple-element.65), channel_id=1, source_target_pairs={{0,2},{1,3},{2,0},{3,1},{4,6},{5,7},{6,4},{7,5},{8,10},{9,11},{10,... | collective-permute-start | bytes 393224 | tf_op jit(solution)/shard_map/ppermute | solution.py:31
  73.0 11.0 %collective-permute-start.17 = (bf16[32,2048]{1,0:T(8,128)(2,1)S(1)}, bf16[32,2048]{1,0:T(8,128)(2,1)S(1)}, u32[]{:S(2)}, u32[]{:S(2)}) collective-permute-start(bf16[32,2048]{1,0:T(8,128)(2,1)S(1)} %get-tuple-element.68), channel_id=1, source_target_pairs={{0,2},{1,3},{2,0},{3,1},{4,6},{5,7},{6,4},{7,5},{8,10},{9,11},{10,... | collective-permute-start | bytes 393224 | tf_op jit(solution)/shard_map/ppermute | solution.py:31
  75.8 9.8 %collective-permute-start.33 = (bf16[16,2048]{1,0:T(8,128)(2,1)S(1)}, bf16[16,2048]{1,0:T(8,128)(2,1)S(1)}, u32[]{:S(2)}, u32[]{:S(2)}) collective-permute-start(bf16[16,2048]{1,0:T(8,128)(2,1)S(1)} %get-tuple-element.80), channel_id=1, source_target_pairs={{0,16},{4,20},{8,24},{12,28},{16,0},{20,4},{24,8},{28,12},{1,17},{... | collective-permute-start | bytes 196616 | tf_op jit(solution)/shard_map/ppermute | solution.py:31
  77.3 9.8 %collective-permute-start.34 = (bf16[16,2048]{1,0:T(8,128)(2,1)S(1)}, bf16[16,2048]{1,0:T(8,128)(2,1)S(1)}, u32[]{:S(2)}, u32[]{:S(2)}) collective-permute-start(bf16[16,2048]{1,0:T(8,128)(2,1)S(1)} %get-tuple-element.81), channel_id=1, source_target_pairs={{0,20},{4,16},{8,28},{12,24},{16,4},{20,0},{24,12},{28,8},{1,21},{... | collective-permute-start | bytes 196616 | tf_op jit(solution)/shard_map/ppermute | solution.py:31
  79.1 8.6 %collective-permute-start.36 = (bf16[16,2048]{1,0:T(8,128)(2,1)S(1)}, bf16[16,2048]{1,0:T(8,128)(2,1)S(1)}, u32[]{:S(2)}, u32[]{:S(2)}) collective-permute-start(bf16[16,2048]{1,0:T(8,128)(2,1)S(1)} %get-tuple-element.83), channel_id=1, source_target_pairs={{0,24},{4,28},{8,16},{12,20},{16,8},{20,12},{24,0},{28,4},{1,25},{... | collective-permute-start | bytes 196616 | tf_op jit(solution)/shard_map/ppermute | solution.py:31
  81.5 7.4 %collective-permute-start.37 = (bf16[16,2048]{1,0:T(8,128)(2,1)S(1)}, bf16[16,2048]{1,0:T(8,128)(2,1)S(1)}, u32[]{:S(2)}, u32[]{:S(2)}) collective-permute-start(bf16[16,2048]{1,0:T(8,128)(2,1)S(1)} %get-tuple-element.84), channel_id=1, source_target_pairs={{0,28},{4,24},{8,20},{12,16},{16,12},{20,8},{24,4},{28,0},{1,29},{... | collective-permute-start | bytes 196616 | tf_op jit(solution)/shard_map/ppermute | solution.py:31
  84.1 5.6 %collective-permute-start.16 = (bf16[16,2048]{1,0:T(8,128)(2,1)S(1)}, bf16[16,2048]{1,0:T(8,128)(2,1)S(1)}, u32[]{:S(2)}, u32[]{:S(2)}) collective-permute-start(bf16[16,2048]{1,0:T(8,128)(2,1)S(1)} %get-tuple-element.67), channel_id=1, source_target_pairs={{0,4},{4,0},{8,12},{12,8},{16,20},{20,16},{24,28},{28,24},{1,5},{5... | collective-permute-start | bytes 196616 | tf_op jit(solution)/shard_map/ppermute | solution.py:31
  85.6 4.3 %collective-permute-start.18 = (bf16[16,2048]{1,0:T(8,128)(2,1)S(1)}, bf16[16,2048]{1,0:T(8,128)(2,1)S(1)}, u32[]{:S(2)}, u32[]{:S(2)}) collective-permute-start(bf16[16,2048]{1,0:T(8,128)(2,1)S(1)} %get-tuple-element.69), channel_id=1, source_target_pairs={{0,8},{4,12},{8,0},{12,4},{16,24},{20,28},{24,16},{28,20},{1,9},{5... | collective-permute-start | bytes 196616 | tf_op jit(solution)/shard_map/ppermute | solution.py:31
  87.2 5.2 %collective-permute-start.19 = (bf16[16,2048]{1,0:T(8,128)(2,1)S(1)}, bf16[16,2048]{1,0:T(8,128)(2,1)S(1)}, u32[]{:S(2)}, u32[]{:S(2)}) collective-permute-start(bf16[16,2048]{1,0:T(8,128)(2,1)S(1)} %get-tuple-element.70), channel_id=1, source_target_pairs={{0,12},{4,8},{8,4},{12,0},{16,28},{20,24},{24,20},{28,16},{1,13},{... | collective-permute-start | bytes 196616 | tf_op jit(solution)/shard_map/ppermute | solution.py:31
  (9 other events, 91.8 us)
